TPU v7x, 128 devices: a whole 4x4x4 slice. The times are simulated.
128 devices in a mesh: sp: 64 (over z, y, x), tp: 2 (over core).
Axes of the slice: x: 4, y: 4, z: 4, core: 2. Of those that a mesh axis runs over, the one named last changes fastest.
Arguments:
- wide_inputs: bfloat16 [8192, 512], P('sp', 'tp'), may hold values from -6 to 6
- narrow_inputs: bfloat16 [8192, 512], P('sp', 'tp'), may hold values from -6 to 6
- wide_poles: float32 [2, 2, 32, 64], P(None, None, 'tp'), may hold values from -3.1416 to 3.1416, as said below
- narrow_poles: float32 [2, 2, 32, 32], P(None, None, 'tp'), may hold values from -3.1416 to 3.1416, as said below
- step_sizes: float32 [2, 2, 32], P(None, None, 'tp'), may hold values from 0 to 1, as said below
- forget: float32 [2, 2, 32, 8192], P(None, None, 'tp', 'sp'), may hold values from 0 to 2.2
- wide_in_map: float32 [2, 2, 32, 16, 64], P(None, None, 'tp'), may hold values from -2.5 to 2.5
- narrow_in_map: float32 [2, 2, 32, 16, 32], P(None, None, 'tp'), may hold values from -2.5 to 2.5
- wide_out_map: float32 [2, 2, 32, 16, 64], P(None, None, 'tp'), may hold values from -1.25 to 1.25
- narrow_out_map: float32 [2, 2, 32, 16, 32], P(None, None, 'tp'), may hold values from -2 to 2
- skip_weight: bfloat16 [2, 512], P(None, 'tp'), may hold values from -6 to 6
- gate_mix: bfloat16 [2, 32, 16, 16], P(None, 'tp'), may hold values from -1.5 to 1.5
- residual: bfloat16 [8192, 2048], P(('sp', 'tp')), may hold values from -6 to 6
- mixer_gain: float32 [1024], replicated, may hold values from 0.1 to 1.9
- out_proj: bfloat16 [1024, 2048], replicated, may hold values from -0.1875 to 0.1875
- ffn_gain: float32 [2048], replicated, may hold values from 0.1 to 1.9
- routes: int32 [8192, 2], P(('sp', 'tp')), may hold values from 0 to 127, all different within a row; in each aligned block of 64 rows (0 to 63, 64 to 127, ...) at most 2 rows name the same one
- route_weights: float32 [8192, 2], P(('sp', 'tp')), may hold values from 0.1 to 1
- gate_proj: bfloat16 [128, 2048, 1408], P(('sp', 'tp')), may hold values from -0.125 to 0.125
- up_proj: bfloat16 [128, 2048, 1408], P(('sp', 'tp')), may hold values from -0.125 to 0.125
- down_proj: bfloat16 [128, 1408, 2048], P(('sp', 'tp')), may hold values from -0.15625 to 0.15625
Outputs:
- layer_out: bfloat16 [8192, 2048], P(('sp', 'tp'))
Inputs may be any that keep to these rules, and one draw needn't show every extreme that they name: `routes`: in each aligned block of 64 rows (the rows of one device), no expert is named by more than 2 entries, and the 2 experts of a row differ. `wide_poles`: along dimension 1, entry 0 (the real part) is negative and entry 1 (the imaginary part) is at least 0.1 in magnitude. `narrow_poles`: along dimension 1, entry 0 (the real part) is negative and entry 1 (the imaginary part) is at least 0.1 in magnitude. `step_sizes`: Positive.
All inputs are finite; a program needn't handle non-finite values.
Results may differ from a plain program's by a relative error of at most 0.014.
Values may be sent and summed in bfloat16 or wider, within the bound.
A program may use at most 192 MiB of HBM per device.

v0:
```python
import functools

import jax
import jax.numpy as jnp
from jax import lax
from jax.experimental import pallas as pl
from jax.experimental.pallas import tpu as pltpu
from jax.sharding import Mesh
from jax.sharding import PartitionSpec as P

SP = ("sp_0", "sp_1", "sp_2")
SP_TP = ("sp_0", "sp_1", "sp_2", "tp")
MESH = pl.DeviceIdType.MESH
epsilon = 1e-06
F32 = jnp.float32
BF16 = jnp.bfloat16
NL = 1536
SETS = ((64, 0), (32, 1024))
CHUNK = 512


def dot(a, b):
    return lax.dot_general(a, b, (((1,), (0,)), ((), ())), preferred_element_type=F32)


def dot_nt(a, b):
    return lax.dot_general(a, b, (((1,), (1,)), ((), ())), preferred_element_type=F32)


def split3(x):
    first = x.astype(BF16)
    rest = x - first.astype(F32)
    second = rest.astype(BF16)
    third = (rest - second.astype(F32)).astype(BF16)
    return first, second, third


def iota(shape, dim):
    return lax.broadcasted_iota(jnp.int32, shape, dim)


def cmul(ar, ai, br, bi):
    return ar * br - ai * bi, ar * bi + ai * br


def square(ar, ai):
    return ar * ar - ai * ai, 2.0 * ar * ai


def mixer_kernel(
    uw_ref, un_ref, pw_ref, pn_ref, step_ref, forget_ref, inw_ref, inn_ref, ow_ref, on_ref,
    skip_ref, gate_ref,
    out_ref,
    win_w, win_n, wout_w, wout_n, xs, es, spread, carry_ref, prod_ref, lam_ref, send, recv, mine,
    send_sem, recv_sem, tp_send, tp_recv,
):
    axes = ("sp_2", "sp_1", "sp_0")
    pos = [lax.axis_index(a) for a in axes]
    core = lax.axis_index("tp")

    barrier = pltpu.get_barrier_semaphore()
    for a, p in zip(axes, pos):
        for o in (1, 2, 3):
            pl.semaphore_signal(barrier, inc=1, device_id={a: lax.rem(p + o, 4)}, device_id_type=MESH)
    pl.semaphore_signal(barrier, inc=1, device_id={"tp": 1 - core}, device_id_type=MESH)

    for s, (p_ref, in_ref, o_ref, win, wout) in enumerate(
        ((pw_ref, inw_ref, ow_ref, win_w, wout_w), (pn_ref, inn_ref, on_ref, win_n, wout_n))
    ):
        n, first = SETS[s]
        tile_r = iota((n, 8 * n), 0)
        tile_c = iota((n, 8 * n), 1)
        tiler = (tile_r == lax.rem(tile_c, n)).astype(BF16)
        wr = iota((128, 8 * n), 0)
        wc = iota((128, 8 * n), 1)
        keep = (wr // 16) == (wc // n)
        for d in range(2):
            pr = p_ref[d, 0]
            pi = p_ref[d, 1]
            grow = jnp.exp(pr)
            lre = grow * jnp.cos(pi)
            lim = grow * jnp.sin(pi)
            nre = lre - 1.0
            scale = step_ref[d, s] / (pr * pr + pi * pi)
            fre = (nre * pr + lim * pi) * scale
            fim = (lim * pr - nre * pi) * scale
            for ri, lam in ((0, lre), (1, lim)):
                parts = jnp.concatenate(split3(lam), axis=0)
                for h in range(2):
                    wide = dot(parts, tiler)
                    gr = lax.rem(iota((48, 8 * n), 0), 16)
                    gc = iota((48, 8 * n), 1) // n + 8 * h
                    row = jnp.sum(jnp.where(gr == gc, wide, 0.0), axis=0, keepdims=True)
                    lam_ref[2 * d + ri : 2 * d + ri + 1, first + 8 * n * h : first + 8 * n * (h + 1)] = row
            ere, eim = [], []
            for g in range(16):
                a = in_ref[d, 0, g * 16 : (g + 1) * 16, :]
                b = in_ref[d, 1, g * 16 : (g + 1) * 16, :]
                fr, fi = fre[g : g + 1], fim[g : g + 1]
                ere.append((fr * a - fi * b).astype(BF16))
                eim.append((fr * b + fi * a).astype(BF16))
            for h in range(2):
                for ri, rows in ((0, ere), (1, eim)):
                    part = jnp.concatenate(rows[8 * h : 8 * h + 8], axis=0)
                    win[d, ri, h] = jnp.where(keep, dot(part, tiler), 0.0).astype(BF16)
                    o = o_ref[d, ri, h * 128 : (h + 1) * 128, :]
                    o = (-o if ri else o).astype(BF16)
                    wout[d, ri, h] = jnp.where(keep, dot(o, tiler), 0.0).astype(BF16)

    pr_ = iota((128, 128), 0)
    pc_ = iota((128, 128), 1)
    perm = (pc_ == lax.rem(pr_, 8) * 16 + pr_ // 8).astype(BF16)
    back = (pr_ == lax.rem(pc_, 8) * 16 + pc_ // 8).astype(BF16)
    u = [dot(perm, uw_ref[...]), dot(perm, un_ref[...])]
    ub = [x.astype(BF16) for x in u]
    for d in range(2):
        for s, win in enumerate((win_w, win_n)):
            n, first = SETS[s]
            for h in range(2):
                at = first + 8 * n * h
                for ri in range(2):
                    xs[d, ri, :, at : at + 8 * n] = dot(ub[s][:, h * 128 : (h + 1) * 128], win[d, ri, h])
    ef = jnp.concatenate(split3(jnp.exp(-forget_ref[...])), axis=0)
    ep = dot_nt(perm, ef).astype(BF16)
    sr = lax.rem(iota((192, NL), 0), 64)
    sc = iota((192, NL), 1)
    group_of = jnp.where(sc < 1024, sc // 64, 16 + (sc - 1024) // 32)
    for d in range(2):
        spread[d] = (sr == group_of + 32 * d).astype(BF16)
        es[d] = dot(ep, spread[d])

    def scan_step(i, state, c, keep_states):
        new = []
        for d in range(2):
            row = i if d == 0 else 15 - i
            at = pl.ds(pl.multiple_of(row * 8, 8), 8)
            lanes = slice(c * CHUNK, (c + 1) * CHUNK)
            lr = lam_ref[2 * d : 2 * d + 1, lanes]
            li = lam_ref[2 * d + 1 : 2 * d + 2, lanes]
            sre, sim = state[3 * d], state[3 * d + 1]
            e = es[d, at, lanes]
            nre = (lr * sre - li * sim) * e + xs[d, 0, at, lanes]
            nim = (lr * sim + li * sre) * e + xs[d, 1, at, lanes]
            if keep_states:
                xs[d, 0, at, lanes] = nre
                xs[d, 1, at, lanes] = nim
            new += [nre, nim, state[3 * d + 2] if keep_states else state[3 * d + 2] * e]
        return tuple(new)

    sub = iota((8, CHUNK), 0)
    ends = [[], []]
    for c in range(NL // CHUNK):
        zero = jnp.zeros((8, CHUNK), F32)
        one = jnp.ones((8, CHUNK), F32)
        state = lax.fori_loop(
            0, 16, lambda i, st: scan_step(i, st, c, False), (zero, zero, one, zero, zero, one)
        )
        lanes = slice(c * CHUNK, (c + 1) * CHUNK)
        for d in range(2):
            sre, sim, g = state[3 * d : 3 * d + 3]
            lr, li = lam_ref[2 * d : 2 * d + 1, lanes], lam_ref[2 * d + 1 : 2 * d + 2, lanes]
            for _ in range(4):
                lr, li = square(lr, li)
            place = sub if d == 0 else 7 - sub
            pre, pim = one, zero
            for k in (1, 2, 4):
                shift = k if d == 0 else 8 - k
                has = place >= k
                before_re = jnp.where(has, pltpu.roll(sre, shift, 0), 0.0) * g
                before_im = jnp.where(has, pltpu.roll(sim, shift, 0), 0.0) * g
                add_re, add_im = cmul(lr, li, before_re, before_im)
                sre, sim = sre + add_re, sim + add_im
                g = g * jnp.where(has, pltpu.roll(g, shift, 0), 1.0)
                tre, tim = cmul(lr, li, pre, pim)
                bit = lax.rem(place // k, 2) == 1
                pre, pim = jnp.where(bit, tre, pre), jnp.where(bit, tim, pim)
                lr, li = square(lr, li)
            edge = 7 if d == 0 else 0
            ends[d].append((sre[edge : edge + 1], sim[edge : edge + 1]))
            shift = 1 if d == 0 else 7
            has = place >= 1
            carry_ref[d, 0, :, lanes] = jnp.where(has, pltpu.roll(sre, shift, 0), 0.0)
            carry_ref[d, 1, :, lanes] = jnp.where(has, pltpu.roll(sim, shift, 0), 0.0)
            gx = jnp.where(has, pltpu.roll(g, shift, 0), 1.0)
            prod_ref[d, 0, :, lanes] = pre * gx
            prod_ref[d, 1, :, lanes] = pim * gx
            lam_ref[4 + 2 * d : 5 + 2 * d, lanes] = lr
            lam_ref[5 + 2 * d : 6 + 2 * d, lanes] = li

    fsum = lax.dot_general(
        jnp.ones((8, 128), F32), forget_ref[...], (((1,), (1,)), ((), ())),
        preferred_element_type=F32, precision=lax.Precision.HIGHEST,
    )[0:1]
    total = [
        [jnp.concatenate([e[q] for e in ends[d]], axis=1) for q in range(2)] for d in range(2)
    ]
    power = [[lam_ref[4 + 2 * d + q : 5 + 2 * d + q, :] for q in range(2)] for d in range(2)]
    enter = None
    pl.semaphore_wait(barrier, 10)
    for stage, a in enumerate(axes):
        p = pos[stage]
        for d in range(2):
            for q in range(2):
                r = 4 * d + 2 * q
                send[stage, r : r + 1, 0:768] = total[d][q][:, 0:768]
                send[stage, r + 1 : r + 2, 0:768] = total[d][q][:, 768:1536]
        send[stage, 0:1, 768:832] = fsum
        copies = []
        for o in (1, 3, 2):
            there = lax.rem(p + o, 4)
            copies.append(
                pltpu.make_async_remote_copy(
                    src_ref=send.at[stage],
                    dst_ref=recv.at[stage, p],
                    send_sem=send_sem.at[stage, o],
                    recv_sem=recv_sem.at[stage, p],
                    device_id={a: there},
                    device_id_type=MESH,
                )
            )
            copies[-1].start()
        for o in (1, 3, 2):
            there = lax.rem(p + o, 4)
            pltpu.make_async_remote_copy(
                src_ref=send.at[stage],
                dst_ref=recv.at[stage, there],
                send_sem=send_sem.at[stage, o],
                recv_sem=recv_sem.at[stage, there],
                device_id={a: there},
                device_id_type=MESH,
            ).wait_recv()
        recv[stage, p] = send[stage]
        sums = jnp.concatenate([recv[stage, k, 0:1, 768:832] for k in range(4)], axis=0)
        parts = jnp.concatenate(split3(jnp.exp(-sums)), axis=1)
        for d in range(2):
            g = dot(parts, spread[d])
            lr, li = power[d]
            rre = rim = jnp.zeros((1, NL), F32)
            ire = iim = jnp.zeros((1, NL), F32)
            are, aim = jnp.ones((1, NL), F32), jnp.zeros((1, NL), F32)
            jre, jim = are, aim
            for step in range(4):
                k = step if d == 0 else 3 - step
                here = k == p
                ire, iim = jnp.where(here, rre, ire), jnp.where(here, rim, iim)
                nearer = (k < p) if d == 0 else (k > p)
                gr, gi = lr * g[k : k + 1], li * g[k : k + 1]
                r = 4 * d
                tre = jnp.concatenate([recv[stage, k, r : r + 1, 0:768], recv[stage, k, r + 1 : r + 2, 0:768]], axis=1)
                tim = jnp.concatenate([recv[stage, k, r + 2 : r + 3, 0:768], recv[stage, k, r + 3 : r + 4, 0:768]], axis=1)
                rre, rim = cmul(gr, gi, rre, rim)
                rre, rim = rre + tre, rim + tim
                nre, nim = cmul(gr, gi, jre, jim)
                jre, jim = jnp.where(nearer, nre, jre), jnp.where(nearer, nim, jim)
            total[d] = [rre, rim]
            lr, li = square(*square(lr, li))
            power[d] = [lr, li]
            if enter is None or len(enter) < 2:
                enter = (enter or []) + [[ire, iim, jre, jim]]
            else:
                bre, bim, cre, cim = enter[d]
                add_re, add_im = cmul(cre, cim, ire, iim)
                ncre, ncim = cmul(cre, cim, jre, jim)
                enter[d] = [bre + add_re, bim + add_im, ncre, ncim]
        fsum = jnp.sum(sums, axis=0, keepdims=True)
        for copy in copies:
            copy.wait_send()

    for c in range(NL // CHUNK):
        lanes = slice(c * CHUNK, (c + 1) * CHUNK)
        state = []
        for d in range(2):
            cre, cim = enter[d][0][:, lanes], enter[d][1][:, lanes]
            add_re, add_im = cmul(prod_ref[d, 0, :, lanes], prod_ref[d, 1, :, lanes], cre, cim)
            state += [carry_ref[d, 0, :, lanes] + add_re, carry_ref[d, 1, :, lanes] + add_im, jnp.zeros((8, 128), F32)]
        lax.fori_loop(0, 16, lambda i, st: scan_step(i, st, c, True), tuple(state))

    for s, wout in enumerate((wout_w, wout_n)):
        n, first = SETS[s]
        for h in range(2):
            at = first + 8 * n * h
            y = None
            for d in range(2):
                for ri in range(2):
                    term = dot_nt(xs[d, ri, :, at : at + 8 * n].astype(BF16), wout[d, ri, h])
                    y = term if y is None else y + term
            ch = slice(h * 128, (h + 1) * 128)
            y = y + skip_ref[s : s + 1, ch].astype(F32) * u[s][:, ch]
            active = jax.nn.gelu(y, approximate=True)
            gr = iota((16, 128), 0)
            gc = iota((16, 128), 1)
            tiler = (gr == lax.rem(gc, 16)).astype(BF16)
            gate = dot(gate_ref[s, ch, :], tiler)
            gate = jnp.where(iota((128, 128), 0) // 16 == iota((128, 128), 1) // 16, gate, 0.0).astype(BF16)
            opened = jax.nn.sigmoid(dot(active.astype(BF16), gate))
            done = dot(back, (active * opened).astype(BF16)).astype(BF16)
            for half in range(2):
                mine[half, :, s * 256 + h * 128 : s * 256 + (h + 1) * 128] = done[half * 64 : (half + 1) * 64]

    copy = pltpu.make_async_remote_copy(
        src_ref=mine.at[1 - core],
        dst_ref=out_ref.at[core],
        send_sem=tp_send,
        recv_sem=tp_recv,
        device_id={"tp": 1 - core},
        device_id_type=MESH,
    )
    copy.start()
    out_ref[core] = mine[core]
    copy.wait()


def mixer(wide_inputs, narrow_inputs, wide_poles, narrow_poles, step_sizes, forget, wide_in_map,
          narrow_in_map, wide_out_map, narrow_out_map, skip_weight, gate_mix):
    vm = pl.BlockSpec(memory_space=pltpu.VMEM)
    return pl.pallas_call(
        mixer_kernel,
        out_shape=jax.ShapeDtypeStruct((2, 64, 512), BF16),
        in_specs=[vm] * 12,
        out_specs=vm,
        scratch_shapes=[
            pltpu.VMEM((2, 2, 2, 128, 512), BF16),
            pltpu.VMEM((2, 2, 2, 128, 256), BF16),
            pltpu.VMEM((2, 2, 2, 128, 512), BF16),
            pltpu.VMEM((2, 2, 2, 128, 256), BF16),
            pltpu.VMEM((2, 2, 128, NL), F32),
            pltpu.VMEM((2, 128, NL), F32),
            pltpu.VMEM((2, 192, NL), BF16),
            pltpu.VMEM((2, 2, 8, NL), F32),
            pltpu.VMEM((2, 2, 8, NL), F32),
            pltpu.VMEM((8, NL), F32),
            pltpu.VMEM((3, 8, 896), F32),
            pltpu.VMEM((3, 4, 8, 896), F32),
            pltpu.VMEM((2, 64, 512), BF16),
            pltpu.SemaphoreType.DMA((3, 4)),
            pltpu.SemaphoreType.DMA((3, 4)),
            pltpu.SemaphoreType.DMA,
            pltpu.SemaphoreType.DMA,
        ],
        compiler_params=pltpu.CompilerParams(
            collective_id=0, has_side_effects=True, vmem_limit_bytes=50 * 1024 * 1024
        ),
        name="mixer",
    )(
        wide_inputs, narrow_inputs, wide_poles, narrow_poles, step_sizes.reshape(2, 2, 16, 1),
        forget.reshape(64, 128),
        wide_in_map.reshape(2, 2, 256, 64), narrow_in_map.reshape(2, 2, 256, 32),
        wide_out_map.reshape(2, 2, 256, 64), narrow_out_map.reshape(2, 2, 256, 32),
        skip_weight, gate_mix.reshape(2, 256, 16),
    )


def in_blocks(shard, dim, count):
    dims = shard.shape
    blocks = shard.reshape(*dims[:dim], count, dims[dim] // count, *dims[dim + 1 :])
    return jnp.moveaxis(blocks, dim, 0)


def one_exchange(blocks):
    return lax.all_to_all(blocks, SP_TP, split_axis=0, concat_axis=0, tiled=True)


def local(
    wide_inputs, narrow_inputs, wide_poles, narrow_poles, step_sizes, forget, wide_in_map,
    narrow_in_map, wide_out_map, narrow_out_map, skip_weight, gate_mix, residual, mixer_gain,
    out_proj, ffn_gain, routes, route_weights, gate_proj, up_proj, down_proj,
):
    parts = mixer(wide_inputs, narrow_inputs, wide_poles, narrow_poles, step_sizes, forget,
                  wide_in_map, narrow_in_map, wide_out_map, narrow_out_map, skip_weight, gate_mix)
    joined = jnp.concatenate(
        [parts[0, :, :256], parts[1, :, :256], parts[0, :, 256:], parts[1, :, 256:]], axis=1
    ).astype(F32)
    scale = lax.rsqrt(jnp.mean(joined * joined, axis=1, keepdims=True) + epsilon)
    mixed = (joined * scale * mixer_gain).astype(BF16)
    projected = jnp.dot(mixed, out_proj, preferred_element_type=F32)
    hidden1 = (residual.astype(F32) + projected).astype(BF16)
    hidden_wide = hidden1.astype(F32)
    normed = (
        hidden_wide
        * lax.rsqrt(jnp.mean(hidden_wide * hidden_wide, axis=1, keepdims=True) + epsilon)
        * ffn_gain
    ).astype(BF16)
    experts, capacity = 128, 2
    width = normed.shape[1]
    picks = routes.reshape(-1)
    onehot = (picks[:, None] == jnp.arange(experts, dtype=jnp.int32)[None, :]).astype(jnp.int32)
    rank = jnp.sum((jnp.cumsum(onehot, axis=0) - onehot) * onehot, axis=1)
    place = picks * capacity + rank
    sectioning = (
        jnp.zeros((experts * capacity, width), BF16).at[place].set(jnp.repeat(normed, 2, axis=0))
    )
    flat_rows = one_exchange(sectioning)
    gate_val = jnp.dot(flat_rows, gate_proj[0], preferred_element_type=F32)
    up_val = jnp.dot(flat_rows, up_proj[0], preferred_element_type=F32)
    expert_hidden = (jax.nn.silu(gate_val) * up_val).astype(BF16)
    done = jnp.dot(expert_hidden, down_proj[0], preferred_element_type=F32).astype(BF16)
    returned = one_exchange(done)
    taken = jnp.take(returned, place, axis=0).reshape(-1, 2, width)
    share = route_weights / jnp.sum(route_weights, axis=1, keepdims=True)
    result = hidden_wide + jnp.sum(share[:, :, None] * taken.astype(F32), axis=1)
    return result.astype(BF16)


def solution(mesh):
    finer = Mesh(mesh.devices.reshape(4, 4, 4, mesh.shape["tp"]), ("sp_0", "sp_1", "sp_2", "tp"))
    return jax.shard_map(
        local,
        mesh=finer,
        in_specs=(
            P(SP, "tp"),
            P(SP, "tp"),
            P(None, None, "tp", None),
            P(None, None, "tp", None),
            P(None, None, "tp"),
            P(None, None, "tp", SP),
            P(None, None, "tp", None, None),
            P(None, None, "tp", None, None),
            P(None, None, "tp", None, None),
            P(None, None, "tp", None, None),
            P(None, "tp"),
            P(None, "tp", None, None),
            P(SP_TP, None),
            P(),
            P(),
            P(),
            P(SP_TP, None),
            P(SP_TP, None),
            P(SP_TP, None, None),
            P(SP_TP, None, None),
            P(SP_TP, None, None),
        ),
        out_specs=P(SP_TP, None),
        check_vma=False,
    )
```

profile of v0, /device:TPU:1, one launch (start us, length us, event | category | flops | bytes accessed | tf_op | source)
XLA Modules:
  0.0 112.6 jit_solution(8850927796706594770)
XLA Ops:
  0.0 0.8 copy.32
  0.8 0.7 broadcast_multiply_fusion
  1.5 0.8 copy.30.step_ref
  2.2 1.0 copy-done
  3.3 1.0 copy-done.1
  4.3 1.0 copy-done.2
  5.4 1.0 copy-done.3
  6.4 0.9 copy-done.4
  7.3 0.8 copy-done.5
  8.2 0.8 copy-done.6
  9.0 0.8 copy-done.7
  9.8 0.8 copy-done.8
  10.5 0.8 copy-done.9
  11.3 0.7 copy-done.10
  11.9 26.5 %mixer.1 = bf16[2,64,512]{2,1,0:T(8,128)(2,1)S(1)} custom-call(bf16[128,256]{1,0:T(8,128)(2,1)S(1)} %copy-done.5, bf16[128,256]{1,0:T(8,128)(2,1)S(1)} %copy-done.6, f32[2,2,16,64]{3,2,1,0:T(8,128)S(1)} %copy-done.7, f32[2,2,16,32]{3,2,1,0:T(8,128)S(1)} %copy-done.8, f32[2,2,16,1]{3,2,1,0:T(8,128)S(1)} %copy.30.step_ref, f32[64,128]{1,0:T(8,128)S(1)} %bitcast.46, ...), custom_call_target="tpu_custom_call" | custom-call | tf_op jit(solution)/shard_map/mixer/pallas_call | solution.py:316
  38.4 0.1 fusion.22
  38.6 3.3 %multiply_reduce_fusion.1 = (f32[64]{0:T(128)S(1)}, f32[64,2048]{1,0:T(8,128)S(1)}) fusion(bf16[1024,2048]{1,0:T(8,128)(2,1)} %param.35, f32[1024]{0:T(1024)} %param.34, f32[64]{0:T(128)S(1)} %add_rsqrt_fusion.1, bf16[64,256]{1,0:T(8,128)(2,1)S(1)} %get-tuple-element.6, bf16[64,256]{1,0:T(8,128)(2,1)S(1)} %get-tuple-element.7, ...), kind=kOutput, calls=%fused_computation.19 | convolution fusion | flops 269942720 | bytes 5116416 | tf_op jit(solution)/shard_map/dot_general | solution.py:375
  41.9 0.0 copy-done.12
  41.9 0.1 multiply_convert_fusion
  42.0 0.3 broadcast_in_dim.26
  42.3 0.2 reshape.115
  42.5 0.1 reshape.101
  42.6 0.1 fusion.28
  42.7 0.2 reduce_window_sum.11
  42.9 0.2 select_reduce_fusion
  43.1 0.1 copy.35
  43.2 0.1 mul.84
  43.4 1.7 %scatter_custom_fusion = bf16[256,2048]{1,0:T(8,128)(2,1)S(1)} fusion(s32[128]{0:T(128)S(1)} %fusion.29, bf16[128,2048]{1,0:T(8,128)(2,1)S(1)} %reshape.115, bf16[]{:T(256)} %constant.36.clone.1), kind=kCustom, calls=%fused_computation.20 | custom fusion | bytes 1048578 | tf_op jit(solution)/shard_map/scatter | solution.py:390
  45.1 0.7 all_to_all.16
  45.8 22.3 %all_to_all.24 = bf16[128,2,2048]{2,1,0:T(2,128)(2,1)S(1)} all-to-all(bf16[128,2,2048]{2,1,0:T(2,128)(2,1)S(1)} %all_to_all.16), channel_id=1, replica_groups=mesh['sp_0'=4,'sp_1'=4,'sp_2'=4,'tp'=2] {'sp_0','sp_1','sp_2','tp'}, dimensions={0} | all-to-all | bytes 2097152 | tf_op jit(solution)/shard_map/all_to_all | solution.py:360
  68.1 0.4 all_to_all.18
  68.5 5.5 %fusion.4 = f32[256,1408]{1,0:T(8,128)} fusion(bf16[256,2048]{1,0:T(8,128)(2,1)S(1)} %all_to_all.18, bf16[1,2048,1408]{2,1,0:T(8,128)(2,1)} %param.39), kind=kOutput, calls=%fused_computation.6 | convolution fusion | flops 1476395008 | bytes 8257536 | tf_op jit(solution)/shard_map/dot_general | solution.py:393
  74.1 8.2 %fusion.12 = bf16[256,2048]{1,0:T(8,128)(2,1)S(1)} fusion(bf16[1,1408,2048]{2,1,0:T(8,128)(2,1)} %param.41, bf16[256,2048]{1,0:T(8,128)(2,1)S(1)} %all_to_all.18, bf16[1,2048,1408]{2,1,0:T(8,128)(2,1)} %param.40, f32[256,1408]{1,0:T(8,128)} %fusion.4), kind=kOutput, calls=%fused_computation.10 | convolution fusion | flops 2955476992 | bytes 15073280 | tf_op jit(solution)/shard_map/dot_general | solution.py:396
  82.3 0.0 copy-start.11
  82.3 0.0 copy-start.13
  82.3 1.5 %all_to_all.19 = bf16[128,2,2048]{2,1,0:T(2,128)(2,1)} reshape(bf16[256,2048]{1,0:T(8,128)(2,1)S(1)} %fusion.12) | data formatting | bytes 2097152 | tf_op jit(solution)/shard_map/all_to_all | solution.py:360
  83.8 4.4 %all-to-all-start.1 = ((bf16[128,2,2048]{2,1,0:T(2,128)(2,1)}), bf16[128,2,2048]{2,1,0:T(2,128)(2,1)S(1)}, u32[]{:S(2)}, u32[]{:S(2)}) async-start(bf16[128,2,2048]{2,1,0:T(2,128)(2,1)} %all_to_all.19), calls=%async_computation.1 | async-start | bytes 2097152 | tf_op jit(solution)/shard_map/all_to_all | solution.py:360
  88.3 0.1 reduce_sum.52
  88.4 0.1 copy.33
  88.5 0.0 copy-done.11
  88.5 0.1 copy.34
  88.6 0.1 copy.31
  88.8 18.8 %all-to-all-done.1 = bf16[128,2,2048]{2,1,0:T(2,128)(2,1)S(1)} async-done(((bf16[128,2,2048]{2,1,0:T(2,128)(2,1)}), bf16[128,2,2048]{2,1,0:T(2,128)(2,1)S(1)}, u32[]{:S(2)}, u32[]{:S(2)}) %all-to-all-start.1) | async-done | bytes 1048608 | tf_op jit(solution)/shard_map/all_to_all | solution.py:360
  107.6 0.4 all_to_all.21
  108.0 0.9 gather_fusion
  108.9 0.3 gather.7
  109.3 2.5 %multiply_reduce_fusion = f32[64,2048]{1,0:T(8,128)S(1)} fusion(bf16[64,2,2048]{2,1,0:T(2,128)(2,1)S(1)} %gather.7, pred[64,2]{1,0:T(8,128)(4,1)S(1)} %copy.34, f32[64,2]{1,0:T(8,128)S(1)} %copy.31), kind=kLoop, calls=%fused_computation.14 | loop fusion | flops 917504 | bytes 1049216 | tf_op jit(solution)/shard_map/reduce_sum | solution.py:400
  111.8 0.8 add_convert_fusion
  (21 shorter events, 0.1 us)
Async XLA Ops:
  0.0 41.9 %copy-start.12 = (f32[2048]{0:T(1024)S(1)}, f32[2048]{0:T(1024)}, u32[]{:S(2)}) copy-start(f32[2048]{0:T(1024)} %param.36) | copy-start | bytes 24580
  2.2 1.0 copy-start
  3.3 1.0 copy-start.1
  4.3 1.0 copy-start.2
  5.4 1.0 copy-start.3
  6.4 0.9 copy-start.4
  7.3 0.8 copy-start.5
  8.2 0.8 copy-start.6
  9.0 0.8 copy-start.7
  9.8 0.8 copy-start.8
  10.5 0.8 copy-start.9
  11.3 0.7 copy-start.10
  82.3 6.2 %copy-start.11 = (s32[64,2]{0,1:T(2,128)S(1)}, s32[64,2]{0,1:T(2,128)}, u32[]{:S(2)}) copy-start(s32[64,2]{0,1:T(2,128)} %param.37) | copy-start | bytes 1540
  82.3 6.3 %copy-start.13 = (f32[64,2]{0,1:T(2,128)S(1)}, f32[64,2]{0,1:T(2,128)}, u32[]{:S(2)}) copy-start(f32[64,2]{0,1:T(2,128)} %param.38) | copy-start | bytes 1540
  83.8 23.8 %all-to-all-start.1 = ((bf16[128,2,2048]{2,1,0:T(2,128)(2,1)}), bf16[128,2,2048]{2,1,0:T(2,128)(2,1)S(1)}, u32[]{:S(2)}, u32[]{:S(2)}) async-start(bf16[128,2,2048]{2,1,0:T(2,128)(2,1)} %all_to_all.19), calls=%async_computation.1 | async-start | bytes 2097152 | tf_op jit(solution)/shard_map/all_to_all | solution.py:360
where the time goes:
time: 113 us
  Pallas kernels  26.5 us (23%)
  blocking collectives  22.3 us (20%)
  waiting for transfers between devices  18.8 us (17%)
  local copies, waits for them, and re-layouts  18.6 us (16%)
  matrix products  17 us (15%)
  other arithmetic  4.72 us (4%)
  starting transfers between devices  4.43 us (4%)
    pallas_call x1, Pallas kernels, mixer(): pl.pallas_call(mixer_kernel, out_shape=jax.ShapeDtypeStruct((2, 64, 512),...  26.5 us
    all_to_all x1, blocking collectives, one_exchange(): lax.all_to_all(blocks, SP_TP, split_axis=0, concat_axis=0, tiled=True)  22.3 us
    all_to_all x1, waiting for transfers between devices, one_exchange(): lax.all_to_all(blocks, SP_TP, split_axis=0, concat_axis=0, tiled=True)  18.8 us
    unnamed x29, local copies, waits for them, and re-layouts  10.5 us
    dot_general x1, matrix products, local(): jnp.dot(expert_hidden, down_proj[0], preferred_element_type=F32)  8.19 us
    dot_general x1, matrix products, local(): gate_val = jnp.dot(flat_rows, gate_proj[0], preferred_element_type=F32)  5.55 us
    all_to_all x1, starting transfers between devices, one_exchange(): lax.all_to_all(blocks, SP_TP, split_axis=0, concat_axis=0, tiled=True)  4.43 us
    dot_general x1, matrix products, local(): projected = jnp.dot(mixed, out_proj, preferred_element_type=F32)  3.25 us
  transfers between devices with their start and end apart: 1, of which 1 were waited for; matrix products, arithmetic and copies ran while one was open for 0% of the time, Pallas kernels for 0%

commit v1 on v0

--- a/solution.py
+++ b/solution.py
@@ -47,22 +47,122 @@
     return ar * ar - ai * ai, 2.0 * ar * ai
 
 
-def mixer_kernel(
-    uw_ref, un_ref, pw_ref, pn_ref, step_ref, forget_ref, inw_ref, inn_ref, ow_ref, on_ref,
-    skip_ref, gate_ref,
-    out_ref,
-    win_w, win_n, wout_w, wout_n, xs, es, spread, carry_ref, prod_ref, lam_ref, send, recv, mine,
-    send_sem, recv_sem, tp_send, tp_recv,
-):
+def coords():
+    return [lax.axis_index(a) for a in SP_TP]
+
+
+def partner(o):
+    o = lax.rem(o * 37, 128)
+    steps = (o // 32, lax.rem(o // 8, 4), lax.rem(o // 2, 4), lax.rem(o, 2))
+    there = [lax.rem(p + s, n) for p, s, n in zip(coords(), steps, (4, 4, 4, 2))]
+    number = ((there[0] * 4 + there[1]) * 4 + there[2]) * 2 + there[3]
+    return dict(zip(SP_TP, there)), number
+
+
+def my_number():
+    z, y, x, c = coords()
+    return ((z * 4 + y) * 4 + x) * 2 + c
+
+
+def to_everyone(out, arrived, send_sem, recv_sem):
+    me = my_number()
+
+    def one(o, carry):
+        where, number = partner(o)
+        pltpu.make_async_remote_copy(
+            src_ref=out.at[number], dst_ref=arrived.at[me], send_sem=send_sem, recv_sem=recv_sem,
+            device_id=where, device_id_type=MESH,
+        ).start()
+        return carry
+
+    lax.fori_loop(1, 128, one, 0)
+    arrived[me] = out[me]
+
+
+def all_of(out, arrived, send_sem, recv_sem):
+    return pltpu.make_async_remote_copy(
+        src_ref=out.at[pl.ds(0, 127)], dst_ref=arrived.at[pl.ds(0, 127)], send_sem=send_sem,
+        recv_sem=recv_sem, device_id={"tp": 1 - lax.axis_index("tp")}, device_id_type=MESH,
+    )
+
+
+def swap_matrix():
+    r, c = iota((256, 256), 0), iota((256, 256), 1)
+    return (lax.rem(r, 16) * 16 + r // 16 == c).astype(BF16)
+
+
+def pack(rows, swap, out):
+    for k in range(4):
+        both = jnp.concatenate(
+            [
+                jnp.concatenate(
+                    [rows(q // 8, 16 * (2 * k + side), q % 8) for q in range(16)], axis=0
+                )
+                for side in range(2)
+            ],
+            axis=1,
+        )
+        done = dot(swap, both).astype(BF16)
+        for side in range(2):
+            at = 16 * (2 * k + side)
+            out[at : at + 16] = done[:, side * 128 : (side + 1) * 128].reshape(16, 16, 128)
+
+
+def unpack(block, swap, put):
+    for k in range(4):
+        both = jnp.concatenate(
+            [block(16 * (2 * k + side)).reshape(256, 128) for side in range(2)], axis=1
+        )
+        done = dot(swap, both).astype(BF16)
+        for side in range(2):
+            at = 16 * (2 * k + side)
+            for q in range(16):
+                put(q // 8, at, q % 8, done[q * 16 : (q + 1) * 16, side * 128 : (side + 1) * 128])
+
+
+def layer_kernel(*refs):
+    ins, out_ref, held = refs[:21], refs[21], refs[22 : 22 + 21]
+    (win_w, win_n, wout_w, wout_n, xs, es, spread, carry_ref, prod_ref, lam_ref, send, recv, mine, theirs,
+     res_out, res_in, mix_out, mix_in, ret_out, ret_in, slots, rows_ref, mixed_ref, hidden_ref, normed_ref, inner_ref,
+     back_ref, own_ref,
+     load_sem, send_sem, recv_sem, tp_send, tp_recv, all_send, all_recv) = refs[43:]
     axes = ("sp_2", "sp_1", "sp_0")
     pos = [lax.axis_index(a) for a in axes]
     core = lax.axis_index("tp")
 
     barrier = pltpu.get_barrier_semaphore()
-    for a, p in zip(axes, pos):
-        for o in (1, 2, 3):
-            pl.semaphore_signal(barrier, inc=1, device_id={a: lax.rem(p + o, 4)}, device_id_type=MESH)
-    pl.semaphore_signal(barrier, inc=1, device_id={"tp": 1 - core}, device_id_type=MESH)
+
+    def greet(o, carry):
+        where, _ = partner(o)
+        pl.semaphore_signal(barrier, inc=1, device_id=where, device_id_type=MESH)
+        return carry
+
+    lax.fori_loop(1, 128, greet, 0)
+    loads = [pltpu.make_async_copy(a, b, load_sem.at[k]) for k, (a, b) in enumerate(zip(ins, held))]
+    order = [12, 16, 2, 3, 4, 6, 7, 8, 9, 0, 1, 5, 10, 11, 13, 15, 17, 14, 18, 19, 20]
+    for k in order:
+        loads[k].start()
+    (uw_ref, un_ref, pw_ref, pn_ref, step_ref, forget_ref, inw_ref, inn_ref, ow_ref, on_ref,
+     skip_ref, gate_ref, residual_ref, mgain_ref, outp_ref, fgain_ref, routes_ref, weights_ref,
+     wg_ref, wu_ref, wd_ref) = held
+    for k in order[:2]:
+        loads[k].wait()
+
+    swap = swap_matrix()
+    earlier = (iota((64, 64), 0) < iota((64, 64), 1)).astype(BF16)
+    named = [(iota((128, 64), 0) == routes_ref[k : k + 1, :]).astype(F32) for k in range(2)]
+    count = named[0] + named[1]
+    rank = dot(count.astype(BF16), earlier)
+    pick = [jnp.where(rank == r, count, 0.0).astype(BF16) for r in range(2)]
+    for half in range(2):
+        for r in range(2):
+            slots[r] = dot(pick[r], residual_ref[:, half * 1024 : (half + 1) * 1024]).astype(BF16)
+        pack(lambda r, at, j: slots[r, at : at + 16, j * 128 : (j + 1) * 128], swap, res_out.at[half])
+    pl.semaphore_wait(barrier, 127)
+    for half in range(2):
+        to_everyone(res_out.at[half], res_in.at[half], all_send.at[half], all_recv.at[half])
+    for k in order[2:14]:
+        loads[k].wait()
 
     for s, (p_ref, in_ref, o_ref, win, wout) in enumerate(
         ((pw_ref, inw_ref, ow_ref, win_w, wout_w), (pn_ref, inn_ref, on_ref, win_n, wout_n))
@@ -81,7 +181,8 @@
             lre = grow * jnp.cos(pi)
             lim = grow * jnp.sin(pi)
             nre = lre - 1.0
-            scale = step_ref[d, s] / (pr * pr + pi * pi)
+            step = jnp.sum(jnp.where(iota((16, 16), 0) == iota((16, 16), 1), step_ref[d, s : s + 1, :], 0.0), axis=1, keepdims=True)
+            scale = step / (pr * pr + pi * pi)
             fre = (nre * pr + lim * pi) * scale
             fim = (lim * pr - nre * pi) * scale
             for ri, lam in ((0, lre), (1, lim)):
@@ -196,7 +297,6 @@
     ]
     power = [[lam_ref[4 + 2 * d + q : 5 + 2 * d + q, :] for q in range(2)] for d in range(2)]
     enter = None
-    pl.semaphore_wait(barrier, 10)
     for stage, a in enumerate(axes):
         p = pos[stage]
         for d in range(2):
@@ -299,65 +399,117 @@
 
     copy = pltpu.make_async_remote_copy(
         src_ref=mine.at[1 - core],
-        dst_ref=out_ref.at[core],
+        dst_ref=theirs,
         send_sem=tp_send,
         recv_sem=tp_recv,
         device_id={"tp": 1 - core},
         device_id_type=MESH,
     )
     copy.start()
-    out_ref[core] = mine[core]
+    for k in order[14:18]:
+        loads[k].wait()
     copy.wait()
 
-
-def mixer(wide_inputs, narrow_inputs, wide_poles, narrow_poles, step_sizes, forget, wide_in_map,
-          narrow_in_map, wide_out_map, narrow_out_map, skip_weight, gate_mix):
-    vm = pl.BlockSpec(memory_space=pltpu.VMEM)
-    return pl.pallas_call(
-        mixer_kernel,
-        out_shape=jax.ShapeDtypeStruct((2, 64, 512), BF16),
-        in_specs=[vm] * 12,
-        out_specs=vm,
-        scratch_shapes=[
-            pltpu.VMEM((2, 2, 2, 128, 512), BF16),
-            pltpu.VMEM((2, 2, 2, 128, 256), BF16),
-            pltpu.VMEM((2, 2, 2, 128, 512), BF16),
-            pltpu.VMEM((2, 2, 2, 128, 256), BF16),
-            pltpu.VMEM((2, 2, 128, NL), F32),
-            pltpu.VMEM((2, 128, NL), F32),
-            pltpu.VMEM((2, 192, NL), BF16),
-            pltpu.VMEM((2, 2, 8, NL), F32),
-            pltpu.VMEM((2, 2, 8, NL), F32),
-            pltpu.VMEM((8, NL), F32),
-            pltpu.VMEM((3, 8, 896), F32),
-            pltpu.VMEM((3, 4, 8, 896), F32),
-            pltpu.VMEM((2, 64, 512), BF16),
-            pltpu.SemaphoreType.DMA((3, 4)),
-            pltpu.SemaphoreType.DMA((3, 4)),
-            pltpu.SemaphoreType.DMA,
-            pltpu.SemaphoreType.DMA,
-        ],
-        compiler_params=pltpu.CompilerParams(
-            collective_id=0, has_side_effects=True, vmem_limit_bytes=50 * 1024 * 1024
-        ),
-        name="mixer",
-    )(
-        wide_inputs, narrow_inputs, wide_poles, narrow_poles, step_sizes.reshape(2, 2, 16, 1),
-        forget.reshape(64, 128),
-        wide_in_map.reshape(2, 2, 256, 64), narrow_in_map.reshape(2, 2, 256, 32),
-        wide_out_map.reshape(2, 2, 256, 64), narrow_out_map.reshape(2, 2, 256, 32),
-        skip_weight, gate_mix.reshape(2, 256, 16),
-    )
-
-
-def in_blocks(shard, dim, count):
-    dims = shard.shape
-    blocks = shard.reshape(*dims[:dim], count, dims[dim] // count, *dims[dim + 1 :])
-    return jnp.moveaxis(blocks, dim, 0)
-
-
-def one_exchange(blocks):
-    return lax.all_to_all(blocks, SP_TP, split_axis=0, concat_axis=0, tiled=True)
+    own, other = mine[core].astype(F32), theirs[...].astype(F32)
+    low = jnp.where(core == 0, own, other)
+    high = jnp.where(core == 0, other, own)
+    joined = jnp.concatenate([low[:, :256], high[:, :256], low[:, 256:], high[:, 256:]], axis=1)
+    scale = lax.rsqrt(jnp.mean(joined * joined, axis=1, keepdims=True) + epsilon)
+    mixed = (joined * scale * mgain_ref[...]).astype(BF16)
+    for r in range(2):
+        slots[r] = dot(pick[r], mixed).astype(BF16)
+    pack(lambda r, at, j: slots[r, at : at + 16, j * 128 : (j + 1) * 128], swap, mix_out)
+    to_everyone(mix_out, mix_in, all_send.at[2], all_recv.at[2])
+
+    for c in range(8):
+        lanes = slice(c * 256, (c + 1) * 256)
+        own_ref[:, lanes] = (
+            residual_ref[:, lanes].astype(F32) + dot(mixed, outp_ref[:, lanes])
+        ).astype(BF16)
+    for half in range(2):
+        all_of(res_out.at[half], res_in.at[half], all_send.at[half], all_recv.at[half]).wait_recv()
+
+        def put(r, at, j, rows):
+            lanes = half * 1024 + j * 128
+            rows_ref[r * 128 + at : r * 128 + at + 16, lanes : lanes + 128] = rows
+
+        unpack(lambda at: res_in[half, at : at + 16], swap, put)
+
+    eye = iota((64, 64), 0) == iota((64, 64), 1)
+    def column(row):
+        return jnp.sum(jnp.where(eye, row, 0.0), axis=1, keepdims=True)
+    experts = iota((64, 128), 1).astype(F32)
+    hits = [(column(routes_ref[k : k + 1, :].astype(F32)) == experts).astype(F32) for k in range(2)]
+    w = [column(weights_ref[k : k + 1, :]) for k in range(2)]
+    both = w[0] + w[1]
+    before = (iota((64, 64), 1) < iota((64, 64), 0)).astype(BF16)
+    ranks = dot(before, (hits[0] + hits[1]).astype(BF16))
+    shares = hits[0] * (w[0] / both) + hits[1] * (w[1] / both)
+    parts = []
+    for r in range(2):
+        share = jnp.where(ranks == r, shares, 0.0)
+        first = share.astype(BF16)
+        parts.append((first, (share - first.astype(F32)).astype(BF16)))
+
+    for k in order[18:]:
+        loads[k].wait()
+    all_of(mix_out, mix_in, all_send.at[2], all_recv.at[2]).wait_recv()
+
+    def put_mixed(r, at, j, rows):
+        mixed_ref[r * 128 + at : r * 128 + at + 16, j * 128 : (j + 1) * 128] = rows
+
+    unpack(lambda at: mix_in[at : at + 16], swap, put_mixed)
+    square_sum = jnp.zeros((256, 1), F32)
+    for c in range(8):
+        lanes = slice(c * 256, (c + 1) * 256)
+        h = (rows_ref[:, lanes].astype(F32) + dot(mixed_ref[...], outp_ref[:, lanes])).astype(BF16)
+        hidden_ref[:, lanes] = h
+        wide = h.astype(F32)
+        square_sum = square_sum + jnp.sum(wide * wide, axis=1, keepdims=True)
+    scale = lax.rsqrt(square_sum / 2048.0 + epsilon)
+    for c in range(8):
+        lanes = slice(c * 256, (c + 1) * 256)
+        normed_ref[:, lanes] = (hidden_ref[:, lanes].astype(F32) * scale * fgain_ref[:, lanes]).astype(BF16)
+
+    def expert_step(lanes):
+        g = dot(normed_ref[...], wg_ref[0, :, lanes])
+        v = dot(normed_ref[...], wu_ref[0, :, lanes])
+        inner_ref[:, lanes] = (jax.nn.silu(g) * v).astype(BF16)
+
+    for c in range(5):
+        expert_step(slice(c * 256, (c + 1) * 256))
+    expert_step(slice(1280, 1408))
+
+    for half in range(2):
+        for c in range(4):
+            lanes = slice(half * 1024 + c * 256, half * 1024 + (c + 1) * 256)
+            y = dot(inner_ref[...], wd_ref[0, :, lanes]).astype(BF16)
+            for r in range(2):
+                slots[r, :, c * 256 : (c + 1) * 256] = y[r * 128 : (r + 1) * 128]
+        pack(lambda r, at, j: slots[r, at : at + 16, j * 128 : (j + 1) * 128], swap, ret_out.at[half])
+        to_everyone(ret_out.at[half], ret_in.at[half], all_send.at[3 + half], all_recv.at[3 + half])
+
+    for half in range(2):
+        all_of(ret_out.at[half], ret_in.at[half], all_send.at[3 + half], all_recv.at[3 + half]).wait_recv()
+
+        def put_back(r, at, j, rows):
+            back_ref[r, at : at + 16, j * 128 : (j + 1) * 128] = rows
+
+        unpack(lambda at: ret_in[half, at : at + 16], swap, put_back)
+        for c in range(4):
+            lanes = slice(c * 256, (c + 1) * 256)
+            to = slice(half * 1024 + c * 256, half * 1024 + (c + 1) * 256)
+            y = None
+            for r in range(2):
+                for part in parts[r]:
+                    term = dot(part, back_ref[r, :, lanes])
+                    y = term if y is None else y + term
+            out_ref[:, to] = (own_ref[:, to].astype(F32) + y).astype(BF16)
+
+    for half in range(2):
+        all_of(res_out.at[half], res_in.at[half], all_send.at[half], all_recv.at[half]).wait_send()
+        all_of(ret_out.at[half], ret_in.at[half], all_send.at[3 + half], all_recv.at[3 + half]).wait_send()
+    all_of(mix_out, mix_in, all_send.at[2], all_recv.at[2]).wait_send()
 
 
 def local(
@@ -365,40 +517,62 @@
     narrow_in_map, wide_out_map, narrow_out_map, skip_weight, gate_mix, residual, mixer_gain,
     out_proj, ffn_gain, routes, route_weights, gate_proj, up_proj, down_proj,
 ):
-    parts = mixer(wide_inputs, narrow_inputs, wide_poles, narrow_poles, step_sizes, forget,
-                  wide_in_map, narrow_in_map, wide_out_map, narrow_out_map, skip_weight, gate_mix)
-    joined = jnp.concatenate(
-        [parts[0, :, :256], parts[1, :, :256], parts[0, :, 256:], parts[1, :, 256:]], axis=1
-    ).astype(F32)
-    scale = lax.rsqrt(jnp.mean(joined * joined, axis=1, keepdims=True) + epsilon)
-    mixed = (joined * scale * mixer_gain).astype(BF16)
-    projected = jnp.dot(mixed, out_proj, preferred_element_type=F32)
-    hidden1 = (residual.astype(F32) + projected).astype(BF16)
-    hidden_wide = hidden1.astype(F32)
-    normed = (
-        hidden_wide
-        * lax.rsqrt(jnp.mean(hidden_wide * hidden_wide, axis=1, keepdims=True) + epsilon)
-        * ffn_gain
-    ).astype(BF16)
-    experts, capacity = 128, 2
-    width = normed.shape[1]
-    picks = routes.reshape(-1)
-    onehot = (picks[:, None] == jnp.arange(experts, dtype=jnp.int32)[None, :]).astype(jnp.int32)
-    rank = jnp.sum((jnp.cumsum(onehot, axis=0) - onehot) * onehot, axis=1)
-    place = picks * capacity + rank
-    sectioning = (
-        jnp.zeros((experts * capacity, width), BF16).at[place].set(jnp.repeat(normed, 2, axis=0))
+    ins = (
+        wide_inputs, narrow_inputs, wide_poles, narrow_poles, step_sizes, forget.reshape(64, 128),
+        wide_in_map.reshape(2, 2, 256, 64), narrow_in_map.reshape(2, 2, 256, 32),
+        wide_out_map.reshape(2, 2, 256, 64), narrow_out_map.reshape(2, 2, 256, 32),
+        skip_weight, gate_mix.reshape(2, 256, 16), residual, mixer_gain.reshape(1, 1024), out_proj,
+        ffn_gain.reshape(1, 2048), routes.T, route_weights.T, gate_proj, up_proj, down_proj,
     )
-    flat_rows = one_exchange(sectioning)
-    gate_val = jnp.dot(flat_rows, gate_proj[0], preferred_element_type=F32)
-    up_val = jnp.dot(flat_rows, up_proj[0], preferred_element_type=F32)
-    expert_hidden = (jax.nn.silu(gate_val) * up_val).astype(BF16)
-    done = jnp.dot(expert_hidden, down_proj[0], preferred_element_type=F32).astype(BF16)
-    returned = one_exchange(done)
-    taken = jnp.take(returned, place, axis=0).reshape(-1, 2, width)
-    share = route_weights / jnp.sum(route_weights, axis=1, keepdims=True)
-    result = hidden_wide + jnp.sum(share[:, :, None] * taken.astype(F32), axis=1)
-    return result.astype(BF16)
+    scratch = [pltpu.VMEM(a.shape, a.dtype) for a in ins]
+    scratch += [
+        pltpu.VMEM((2, 2, 2, 128, 512), BF16),
+        pltpu.VMEM((2, 2, 2, 128, 256), BF16),
+        pltpu.VMEM((2, 2, 2, 128, 512), BF16),
+        pltpu.VMEM((2, 2, 2, 128, 256), BF16),
+        pltpu.VMEM((2, 2, 128, NL), F32),
+        pltpu.VMEM((2, 128, NL), F32),
+        pltpu.VMEM((2, 192, NL), BF16),
+        pltpu.VMEM((2, 2, 8, NL), F32),
+        pltpu.VMEM((2, 2, 8, NL), F32),
+        pltpu.VMEM((8, NL), F32),
+        pltpu.VMEM((3, 8, 896), F32),
+        pltpu.VMEM((3, 4, 8, 896), F32),
+        pltpu.VMEM((2, 64, 512), BF16),
+        pltpu.VMEM((64, 512), BF16),
+        pltpu.VMEM((2, 128, 16, 128), BF16),
+        pltpu.VMEM((2, 128, 16, 128), BF16),
+        pltpu.VMEM((128, 16, 128), BF16),
+        pltpu.VMEM((128, 16, 128), BF16),
+        pltpu.VMEM((2, 128, 16, 128), BF16),
+        pltpu.VMEM((2, 128, 16, 128), BF16),
+        pltpu.VMEM((2, 128, 1024), BF16),
+        pltpu.VMEM((256, 2048), BF16),
+        pltpu.VMEM((256, 1024), BF16),
+        pltpu.VMEM((256, 2048), BF16),
+        pltpu.VMEM((256, 2048), BF16),
+        pltpu.VMEM((256, 1408), BF16),
+        pltpu.VMEM((2, 128, 1024), BF16),
+        pltpu.VMEM((64, 2048), BF16),
+        pltpu.SemaphoreType.DMA((21,)),
+        pltpu.SemaphoreType.DMA((3, 4)),
+        pltpu.SemaphoreType.DMA((3, 4)),
+        pltpu.SemaphoreType.DMA,
+        pltpu.SemaphoreType.DMA,
+        pltpu.SemaphoreType.DMA((5,)),
+        pltpu.SemaphoreType.DMA((5,)),
+    ]
+    return pl.pallas_call(
+        layer_kernel,
+        out_shape=jax.ShapeDtypeStruct((64, 2048), BF16),
+        in_specs=[pl.BlockSpec(memory_space=pl.ANY)] * 21,
+        out_specs=pl.BlockSpec(memory_space=pltpu.VMEM),
+        scratch_shapes=scratch,
+        compiler_params=pltpu.CompilerParams(
+            collective_id=0, has_side_effects=True, vmem_limit_bytes=60 * 1024 * 1024
+        ),
+        name="layer",
+    )(*ins)
 
 
 def solution(mesh):

time: 113 us -> 78.4 us (0.69)
  Pallas kernels: 26.5 us -> 76.6 us
  blocking collectives: 22.3 us -> 0 us
  waiting for transfers between devices: 18.8 us -> 0 us
  matrix products: 17 us -> 0 us
  local copies, waits for them, and re-layouts: 18.6 us -> 1.67 us
  other arithmetic: 4.72 us -> 0 us
  starting transfers between devices: 4.43 us -> 0 us
    pallas_call x1, Pallas kernels: 26.5 us -> 76.6 us  [local(): pl.pallas_call(layer_kernel, out_shape=jax.ShapeDtypeStruct((64, 2048), B...]
    all_to_all x1 -> x0, blocking collectives: 22.3 us -> none  [one_exchange(): lax.all_to_all(blocks, SP_TP, split_axis=0, concat_axis=0, tiled=True)]
    all_to_all x1 -> x0, waiting for transfers between devices: 18.8 us -> none  [one_exchange(): lax.all_to_all(blocks, SP_TP, split_axis=0, concat_axis=0, tiled=True)]
    dot_general x3 -> x0, matrix products: 17 us -> none  [the longest x1 8.19 us: local(): jnp.dot(expert_hidden, down_proj[0], preferred_element_type=F32)]
    unnamed x29 -> x1, local copies, waits for them, and re-layouts: 10.5 us -> 1.67 us
    all_to_all x1 -> x0, starting transfers between devices: 4.43 us -> none  [one_exchange(): lax.all_to_all(blocks, SP_TP, split_axis=0, concat_axis=0, tiled=True)]
    all_to_all x4 -> x0, local copies, waits for them, and re-layouts: 3.07 us -> none  [one_exchange(): lax.all_to_all(blocks, SP_TP, split_axis=0, concat_axis=0, tiled=True)]
    reduce_sum x4 -> x0, other arithmetic: 2.85 us -> none  [the longest x1 2.53 us: local(): jnp.sum(share[:, :, None] * taken.astype(F32), axis=1)]
  transfers between devices with their start and end apart: 1 -> 0, of which waited for: 1 -> 0; matrix products, arithmetic and copies ran while one was open for 0% -> 0% of each run, Pallas kernels for 0% -> 0%
where the time goes in v1:
time: 78.4 us; the launch traced here: 78.3 us
  Pallas kernels  76.6 us (98%)
  local copies, waits for them, and re-layouts  1.67 us (2%)
    pallas_call x1, Pallas kernels, local(): pl.pallas_call(layer_kernel, out_shape=jax.ShapeDtypeStruct((64, 2048), B...  76.6 us
    unnamed x1, local copies, waits for them, and re-layouts  1.67 us

profile of v1, /device:TPU:1, one launch (start us, length us, event | category | flops | bytes accessed | tf_op | source)
XLA Modules:
  0.0 78.3 jit_solution(14939509551818859914)
XLA Ops:
  0.0 76.6 %layer.1 = bf16[64,2048]{1,0:T(8,128)(2,1)} custom-call(bf16[128,256]{1,0:T(8,128)(2,1)} %refs_0_.1, bf16[128,256]{1,0:T(8,128)(2,1)} %refs_1_.1, f32[2,2,16,64]{3,2,1,0:T(8,128)} %refs_2_.1, f32[2,2,16,32]{3,2,1,0:T(8,128)} %refs_3_.1, f32[2,2,16]{2,1,0:T(2,128)} %refs_4_.1, f32[64,128]{1,0:T(8,128)} %bitcast.15, f32[2,2,256,64]{3,2,1,0:T(8,128)} %bitcast.10, ...), custom_call_target="tpu_custom_call" | custom-call | tf_op jit(solution)/shard_map/layer/pallas_call | solution.py:565
  76.6 1.7 %copy.23 = bf16[64,2048]{1,0:T(8,128)(2,1)} copy(bf16[64,2048]{1,0:T(8,128)(2,1)} %layer.1) | data formatting | bytes 524288

commit v2 on v1

--- a/solution.py
+++ b/solution.py
@@ -17,6 +17,8 @@
 NL = 1536
 SETS = ((64, 0), (32, 1024))
 CHUNK = 512
+BATCHES = ((1, 31), (31, 61), (61, 91), (91, 128))
+PARTS = ((0, 64), (64, 128))
 
 
 def dot(a, b):
@@ -51,38 +53,44 @@
     return [lax.axis_index(a) for a in SP_TP]
 
 
-def partner(o):
+def partner(o, way=1):
     o = lax.rem(o * 37, 128)
     steps = (o // 32, lax.rem(o // 8, 4), lax.rem(o // 2, 4), lax.rem(o, 2))
-    there = [lax.rem(p + s, n) for p, s, n in zip(coords(), steps, (4, 4, 4, 2))]
+    sizes = (4, 4, 4, 2)
+    there = [lax.rem(p + n + way * s, n) for p, s, n in zip(coords(), steps, sizes)]
     number = ((there[0] * 4 + there[1]) * 4 + there[2]) * 2 + there[3]
     return dict(zip(SP_TP, there)), number
 
 
-def my_number():
-    z, y, x, c = coords()
-    return ((z * 4 + y) * 4 + x) * 2 + c
-
-
-def to_everyone(out, arrived, send_sem, recv_sem):
-    me = my_number()
-
+def send_some(first, last, out, arrived, send_sem, recv_sem):
     def one(o, carry):
-        where, number = partner(o)
+        where, _ = partner(o)
         pltpu.make_async_remote_copy(
-            src_ref=out.at[number], dst_ref=arrived.at[me], send_sem=send_sem, recv_sem=recv_sem,
+            src_ref=out.at[o], dst_ref=arrived.at[o], send_sem=send_sem, recv_sem=recv_sem,
             device_id=where, device_id_type=MESH,
         ).start()
         return carry
 
-    lax.fori_loop(1, 128, one, 0)
-    arrived[me] = out[me]
-
-
-def all_of(out, arrived, send_sem, recv_sem):
+    lax.fori_loop(first, last, one, 0)
+
+
+def send_back(first, last, out, arrived, send_sem, recv_sem):
+    def one(o, carry):
+        where, _ = partner(o, -1)
+        pltpu.make_async_remote_copy(
+            src_ref=out.at[o], dst_ref=arrived.at[o], send_sem=send_sem, recv_sem=recv_sem,
+            device_id=where, device_id_type=MESH,
+        ).start()
+        return carry
+
+    lax.fori_loop(first, last, one, 0)
+
+
+def all_of(first, last, out, arrived, send_sem, recv_sem):
     return pltpu.make_async_remote_copy(
-        src_ref=out.at[pl.ds(0, 127)], dst_ref=arrived.at[pl.ds(0, 127)], send_sem=send_sem,
-        recv_sem=recv_sem, device_id={"tp": 1 - lax.axis_index("tp")}, device_id_type=MESH,
+        src_ref=out.at[pl.ds(first, last - first)], dst_ref=arrived.at[pl.ds(first, last - first)],
+        send_sem=send_sem, recv_sem=recv_sem, device_id={"tp": 1 - lax.axis_index("tp")},
+        device_id_type=MESH,
     )
 
 
@@ -91,33 +99,29 @@
     return (lax.rem(r, 16) * 16 + r // 16 == c).astype(BF16)
 
 
-def pack(rows, swap, out):
-    for k in range(4):
+def pack(rows, swap, put, blocks):
+    for k in range(0, blocks, 32):
         both = jnp.concatenate(
             [
-                jnp.concatenate(
-                    [rows(q // 8, 16 * (2 * k + side), q % 8) for q in range(16)], axis=0
-                )
+                jnp.concatenate([rows(q // 8, k + 16 * side, q % 8) for q in range(16)], axis=0)
                 for side in range(2)
             ],
             axis=1,
         )
         done = dot(swap, both).astype(BF16)
         for side in range(2):
-            at = 16 * (2 * k + side)
-            out[at : at + 16] = done[:, side * 128 : (side + 1) * 128].reshape(16, 16, 128)
-
-
-def unpack(block, swap, put):
-    for k in range(4):
+            put(k + 16 * side, done[:, side * 128 : (side + 1) * 128].reshape(16, 16, 128))
+
+
+def unpack(block, swap, put, blocks):
+    for k in range(0, blocks, 32):
         both = jnp.concatenate(
-            [block(16 * (2 * k + side)).reshape(256, 128) for side in range(2)], axis=1
+            [block(k + 16 * side).reshape(256, 128) for side in range(2)], axis=1
         )
         done = dot(swap, both).astype(BF16)
         for side in range(2):
-            at = 16 * (2 * k + side)
             for q in range(16):
-                put(q // 8, at, q % 8, done[q * 16 : (q + 1) * 16, side * 128 : (side + 1) * 128])
+                put(q // 8, k + 16 * side, q % 8, done[q * 16 : (q + 1) * 16, side * 128 : (side + 1) * 128])
 
 
 def layer_kernel(*refs):
@@ -125,44 +129,49 @@
     (win_w, win_n, wout_w, wout_n, xs, es, spread, carry_ref, prod_ref, lam_ref, send, recv, mine, theirs,
      res_out, res_in, mix_out, mix_in, ret_out, ret_in, slots, rows_ref, mixed_ref, hidden_ref, normed_ref, inner_ref,
      back_ref, own_ref,
-     load_sem, send_sem, recv_sem, tp_send, tp_recv, all_send, all_recv) = refs[43:]
+     load_sem, send_sem, recv_sem, tp_send, tp_recv, all_send, all_recv, known_sem) = refs[43:]
     axes = ("sp_2", "sp_1", "sp_0")
     pos = [lax.axis_index(a) for a in axes]
     core = lax.axis_index("tp")
 
     barrier = pltpu.get_barrier_semaphore()
 
-    def greet(o, carry):
-        where, _ = partner(o)
-        pl.semaphore_signal(barrier, inc=1, device_id=where, device_id_type=MESH)
-        return carry
-
-    lax.fori_loop(1, 128, greet, 0)
+    def greet(semaphore, axis, place, size):
+        for o in range(1, size):
+            pl.semaphore_signal(semaphore, inc=1, device_id={axis: lax.rem(place + o, size)}, device_id_type=MESH)
+
+    for a, p in zip(axes, pos):
+        greet(barrier, a, p, 4)
+    greet(barrier, "tp", core, 2)
     loads = [pltpu.make_async_copy(a, b, load_sem.at[k]) for k, (a, b) in enumerate(zip(ins, held))]
     order = [12, 16, 2, 3, 4, 6, 7, 8, 9, 0, 1, 5, 10, 11, 13, 15, 17, 14, 18, 19, 20]
-    for k in order:
+    for k in order[:17]:
         loads[k].start()
     (uw_ref, un_ref, pw_ref, pn_ref, step_ref, forget_ref, inw_ref, inn_ref, ow_ref, on_ref,
      skip_ref, gate_ref, residual_ref, mgain_ref, outp_ref, fgain_ref, routes_ref, weights_ref,
      wg_ref, wu_ref, wd_ref) = held
-    for k in order[:2]:
+    for k in order[:17]:
         loads[k].wait()
+    for k in order[17:]:
+        loads[k].start()
 
     swap = swap_matrix()
     earlier = (iota((64, 64), 0) < iota((64, 64), 1)).astype(BF16)
-    named = [(iota((128, 64), 0) == routes_ref[k : k + 1, :]).astype(F32) for k in range(2)]
+    expert = partner(iota((128, 64), 0))[1]
+    named = [(expert == routes_ref[k : k + 1, :]).astype(F32) for k in range(2)]
     count = named[0] + named[1]
     rank = dot(count.astype(BF16), earlier)
     pick = [jnp.where(rank == r, count, 0.0).astype(BF16) for r in range(2)]
     for half in range(2):
         for r in range(2):
             slots[r] = dot(pick[r], residual_ref[:, half * 1024 : (half + 1) * 1024]).astype(BF16)
-        pack(lambda r, at, j: slots[r, at : at + 16, j * 128 : (j + 1) * 128], swap, res_out.at[half])
-    pl.semaphore_wait(barrier, 127)
-    for half in range(2):
-        to_everyone(res_out.at[half], res_in.at[half], all_send.at[half], all_recv.at[half])
-    for k in order[2:14]:
-        loads[k].wait()
+
+        def put_residual(at, block):
+            res_out[at : at + 16, half] = block
+
+        pack(lambda r, at, j: slots[r, at : at + 16, j * 128 : (j + 1) * 128], swap, put_residual, 128)
+    pl.semaphore_wait(barrier, 10)
+    greet(known_sem.at[0], "sp_2", pos[0], 4)
 
     for s, (p_ref, in_ref, o_ref, win, wout) in enumerate(
         ((pw_ref, inw_ref, ow_ref, win_w, wout_w), (pn_ref, inn_ref, on_ref, win_n, wout_n))
@@ -208,6 +217,8 @@
                     o = (-o if ri else o).astype(BF16)
                     wout[d, ri, h] = jnp.where(keep, dot(o, tiler), 0.0).astype(BF16)
 
+    pl.semaphore_wait(known_sem.at[0], 3)
+    greet(known_sem.at[1], "sp_1", pos[1], 4)
     pr_ = iota((128, 128), 0)
     pc_ = iota((128, 128), 1)
     perm = (pc_ == lax.rem(pr_, 8) * 16 + pr_ // 8).astype(BF16)
@@ -248,6 +259,8 @@
             new += [nre, nim, state[3 * d + 2] if keep_states else state[3 * d + 2] * e]
         return tuple(new)
 
+    pl.semaphore_wait(known_sem.at[1], 3)
+    greet(known_sem.at[2], "tp", core, 2)
     sub = iota((8, CHUNK), 0)
     ends = [[], []]
     for c in range(NL // CHUNK):
@@ -297,14 +310,16 @@
     ]
     power = [[lam_ref[4 + 2 * d + q : 5 + 2 * d + q, :] for q in range(2)] for d in range(2)]
     enter = None
+    pl.semaphore_wait(known_sem.at[2], 1)
     for stage, a in enumerate(axes):
         p = pos[stage]
-        for d in range(2):
-            for q in range(2):
-                r = 4 * d + 2 * q
-                send[stage, r : r + 1, 0:768] = total[d][q][:, 0:768]
-                send[stage, r + 1 : r + 2, 0:768] = total[d][q][:, 768:1536]
-        send[stage, 0:1, 768:832] = fsum
+        lines = [
+            total[d][q][:, 384 * k : 384 * (k + 1)] for d in range(2) for q in range(2) for k in range(4)
+        ]
+        sums_sent = [x.astype(F32) for x in split3(fsum)] + [jnp.zeros((1, 64), F32)] * 13
+        send[stage] = jnp.concatenate(
+            [jnp.concatenate(lines, axis=0), jnp.concatenate(sums_sent, axis=0)], axis=1
+        ).astype(BF16)
         copies = []
         for o in (1, 3, 2):
             there = lax.rem(p + o, 4)
@@ -319,6 +334,7 @@
                 )
             )
             copies[-1].start()
+        send_some(*BATCHES[stage], res_out, res_in, all_send.at[0], all_recv.at[0])
         for o in (1, 3, 2):
             there = lax.rem(p + o, 4)
             pltpu.make_async_remote_copy(
@@ -330,7 +346,10 @@
                 device_id_type=MESH,
             ).wait_recv()
         recv[stage, p] = send[stage]
-        sums = jnp.concatenate([recv[stage, k, 0:1, 768:832] for k in range(4)], axis=0)
+        came = [recv[stage, k].astype(F32) for k in range(4)]
+        sums = jnp.concatenate(
+            [jnp.sum(x[0:3, 384:448], axis=0, keepdims=True) for x in came], axis=0
+        )
         parts = jnp.concatenate(split3(jnp.exp(-sums)), axis=1)
         for d in range(2):
             g = dot(parts, spread[d])
@@ -345,9 +364,10 @@
                 ire, iim = jnp.where(here, rre, ire), jnp.where(here, rim, iim)
                 nearer = (k < p) if d == 0 else (k > p)
                 gr, gi = lr * g[k : k + 1], li * g[k : k + 1]
-                r = 4 * d
-                tre = jnp.concatenate([recv[stage, k, r : r + 1, 0:768], recv[stage, k, r + 1 : r + 2, 0:768]], axis=1)
-                tim = jnp.concatenate([recv[stage, k, r + 2 : r + 3, 0:768], recv[stage, k, r + 3 : r + 4, 0:768]], axis=1)
+                tre, tim = (
+                    jnp.concatenate([came[k][r : r + 1, 0:384] for r in range(at, at + 4)], axis=1)
+                    for at in (8 * d, 8 * d + 4)
+                )
                 rre, rim = cmul(gr, gi, rre, rim)
                 rre, rim = rre + tre, rim + tim
                 nre, nim = cmul(gr, gi, jre, jim)
@@ -366,6 +386,8 @@
         for copy in copies:
             copy.wait_send()
 
+    send_some(*BATCHES[3], res_out, res_in, all_send.at[0], all_recv.at[0])
+    res_in[0] = res_out[0]
     for c in range(NL // CHUNK):
         lanes = slice(c * CHUNK, (c + 1) * CHUNK)
         state = []
@@ -406,8 +428,6 @@
         device_id_type=MESH,
     )
     copy.start()
-    for k in order[14:18]:
-        loads[k].wait()
     copy.wait()
 
     own, other = mine[core].astype(F32), theirs[...].astype(F32)
@@ -418,27 +438,35 @@
     mixed = (joined * scale * mgain_ref[...]).astype(BF16)
     for r in range(2):
         slots[r] = dot(pick[r], mixed).astype(BF16)
-    pack(lambda r, at, j: slots[r, at : at + 16, j * 128 : (j + 1) * 128], swap, mix_out)
-    to_everyone(mix_out, mix_in, all_send.at[2], all_recv.at[2])
-
+
+    def put_mixed_out(at, block):
+        mix_out[at : at + 16] = block
+
+    pack(lambda r, at, j: slots[r, at : at + 16, j * 128 : (j + 1) * 128], swap, put_mixed_out, 128)
+    for n, (first, last) in enumerate(PARTS):
+        send_some(max(first, 1), last, mix_out, mix_in, all_send.at[1 + n], all_recv.at[1 + n])
+    mix_in[0] = mix_out[0]
+
+    loads[14].wait()
     for c in range(8):
         lanes = slice(c * 256, (c + 1) * 256)
         own_ref[:, lanes] = (
             residual_ref[:, lanes].astype(F32) + dot(mixed, outp_ref[:, lanes])
         ).astype(BF16)
-    for half in range(2):
-        all_of(res_out.at[half], res_in.at[half], all_send.at[half], all_recv.at[half]).wait_recv()
-
-        def put(r, at, j, rows):
-            lanes = half * 1024 + j * 128
-            rows_ref[r * 128 + at : r * 128 + at + 16, lanes : lanes + 128] = rows
-
-        unpack(lambda at: res_in[half, at : at + 16], swap, put)
+    all_of(1, 128, res_out, res_in, all_send.at[0], all_recv.at[0]).wait_recv()
+    for n, (first, last) in enumerate(PARTS):
+        for half in range(2):
+
+            def put_rows(r, at, j, rows):
+                lanes = half * 1024 + j * 128
+                rows_ref[n, r * 64 + at : r * 64 + at + 16, lanes : lanes + 128] = rows
+
+            unpack(lambda at: res_in[first + at : first + at + 16, half], swap, put_rows, 64)
 
     eye = iota((64, 64), 0) == iota((64, 64), 1)
     def column(row):
         return jnp.sum(jnp.where(eye, row, 0.0), axis=1, keepdims=True)
-    experts = iota((64, 128), 1).astype(F32)
+    experts = partner(iota((64, 128), 1))[1].astype(F32)
     hits = [(column(routes_ref[k : k + 1, :].astype(F32)) == experts).astype(F32) for k in range(2)]
     w = [column(weights_ref[k : k + 1, :]) for k in range(2)]
     both = w[0] + w[1]
@@ -453,63 +481,81 @@
 
     for k in order[18:]:
         loads[k].wait()
-    all_of(mix_out, mix_in, all_send.at[2], all_recv.at[2]).wait_recv()
-
-    def put_mixed(r, at, j, rows):
-        mixed_ref[r * 128 + at : r * 128 + at + 16, j * 128 : (j + 1) * 128] = rows
-
-    unpack(lambda at: mix_in[at : at + 16], swap, put_mixed)
-    square_sum = jnp.zeros((256, 1), F32)
+    for n, (first, last) in enumerate(PARTS):
+        all_of(max(first, 1), last, mix_out, mix_in, all_send.at[1 + n], all_recv.at[1 + n]).wait_recv()
+
+        def put_mixed(r, at, j, rows):
+            mixed_ref[r * 64 + at : r * 64 + at + 16, j * 128 : (j + 1) * 128] = rows
+
+        unpack(lambda at: mix_in[first + at : first + at + 16], swap, put_mixed, 64)
+        square_sum = jnp.zeros((128, 1), F32)
+        for c in range(8):
+            lanes = slice(c * 256, (c + 1) * 256)
+            h = (rows_ref[n, :, lanes].astype(F32) + dot(mixed_ref[...], outp_ref[:, lanes])).astype(BF16)
+            hidden_ref[:, lanes] = h
+            wide = h.astype(F32)
+            square_sum = square_sum + jnp.sum(wide * wide, axis=1, keepdims=True)
+        scale = lax.rsqrt(square_sum / 2048.0 + epsilon)
+        for c in range(8):
+            lanes = slice(c * 256, (c + 1) * 256)
+            normed_ref[:, lanes] = (hidden_ref[:, lanes].astype(F32) * scale * fgain_ref[:, lanes]).astype(BF16)
+
+        def expert_step(lanes):
+            g = dot(normed_ref[...], wg_ref[0, :, lanes])
+            v = dot(normed_ref[...], wu_ref[0, :, lanes])
+            inner_ref[:, lanes] = (jax.nn.silu(g) * v).astype(BF16)
+
+        for c in range(5):
+            expert_step(slice(c * 256, (c + 1) * 256))
+        expert_step(slice(1280, 1408))
+
+        for half in range(2):
+            for c in range(4):
+                lanes = slice(half * 1024 + c * 256, half * 1024 + (c + 1) * 256)
+                y = dot(inner_ref[...], wd_ref[0, :, lanes]).astype(BF16)
+                for r in range(2):
+                    slots[r, 0:64, c * 256 : (c + 1) * 256] = y[r * 64 : (r + 1) * 64]
+
+            def put_return(at, block):
+                ret_out[half, first + at : first + at + 16] = block
+
+            pack(lambda r, at, j: slots[r, at : at + 16, j * 128 : (j + 1) * 128], swap, put_return, 64)
+            send_back(
+                max(first, 1), last, ret_out.at[half], ret_in.at[half], all_send.at[3 + 2 * n + half],
+                all_recv.at[3 + 2 * n + half],
+            )
+    for half in range(2):
+        ret_in[half, 0] = ret_out[half, 0]
+
+    y = [own_ref[:, c * 256 : (c + 1) * 256].astype(F32) for c in range(8)]
+    for n, (first, last) in enumerate(PARTS):
+        for half in range(2):
+            all_of(
+                max(first, 1), last, ret_out.at[half], ret_in.at[half], all_send.at[3 + 2 * n + half],
+                all_recv.at[3 + 2 * n + half],
+            ).wait_recv()
+
+            def put_back(r, at, j, rows):
+                back_ref[r, at : at + 16, j * 128 : (j + 1) * 128] = rows
+
+            unpack(lambda at: ret_in[half, first + at : first + at + 16], swap, put_back, 64)
+            for c in range(4):
+                lanes = slice(c * 256, (c + 1) * 256)
+                for r in range(2):
+                    for part in parts[r]:
+                        y[4 * half + c] = y[4 * half + c] + dot(part[:, first:last], back_ref[r, :, lanes])
     for c in range(8):
-        lanes = slice(c * 256, (c + 1) * 256)
-        h = (rows_ref[:, lanes].astype(F32) + dot(mixed_ref[...], outp_ref[:, lanes])).astype(BF16)
-        hidden_ref[:, lanes] = h
-        wide = h.astype(F32)
-        square_sum = square_sum + jnp.sum(wide * wide, axis=1, keepdims=True)
-    scale = lax.rsqrt(square_sum / 2048.0 + epsilon)
-    for c in range(8):
-        lanes = slice(c * 256, (c + 1) * 256)
-        normed_ref[:, lanes] = (hidden_ref[:, lanes].astype(F32) * scale * fgain_ref[:, lanes]).astype(BF16)
-
-    def expert_step(lanes):
-        g = dot(normed_ref[...], wg_ref[0, :, lanes])
-        v = dot(normed_ref[...], wu_ref[0, :, lanes])
-        inner_ref[:, lanes] = (jax.nn.silu(g) * v).astype(BF16)
-
-    for c in range(5):
-        expert_step(slice(c * 256, (c + 1) * 256))
-    expert_step(slice(1280, 1408))
-
-    for half in range(2):
-        for c in range(4):
-            lanes = slice(half * 1024 + c * 256, half * 1024 + (c + 1) * 256)
-            y = dot(inner_ref[...], wd_ref[0, :, lanes]).astype(BF16)
-            for r in range(2):
-                slots[r, :, c * 256 : (c + 1) * 256] = y[r * 128 : (r + 1) * 128]
-        pack(lambda r, at, j: slots[r, at : at + 16, j * 128 : (j + 1) * 128], swap, ret_out.at[half])
-        to_everyone(ret_out.at[half], ret_in.at[half], all_send.at[3 + half], all_recv.at[3 + half])
-
-    for half in range(2):
-        all_of(ret_out.at[half], ret_in.at[half], all_send.at[3 + half], all_recv.at[3 + half]).wait_recv()
-
-        def put_back(r, at, j, rows):
-            back_ref[r, at : at + 16, j * 128 : (j + 1) * 128] = rows
-
-        unpack(lambda at: ret_in[half, at : at + 16], swap, put_back)
-        for c in range(4):
-            lanes = slice(c * 256, (c + 1) * 256)
-            to = slice(half * 1024 + c * 256, half * 1024 + (c + 1) * 256)
-            y = None
-            for r in range(2):
-                for part in parts[r]:
-                    term = dot(part, back_ref[r, :, lanes])
-                    y = term if y is None else y + term
-            out_ref[:, to] = (own_ref[:, to].astype(F32) + y).astype(BF16)
-
-    for half in range(2):
-        all_of(res_out.at[half], res_in.at[half], all_send.at[half], all_recv.at[half]).wait_send()
-        all_of(ret_out.at[half], ret_in.at[half], all_send.at[3 + half], all_recv.at[3 + half]).wait_send()
-    all_of(mix_out, mix_in, all_send.at[2], all_recv.at[2]).wait_send()
+        out_ref[:, c * 256 : (c + 1) * 256] = y[c].astype(BF16)
+
+    all_of(1, 128, res_out, res_in, all_send.at[0], all_recv.at[0]).wait_send()
+    for n, (first, last) in enumerate(PARTS):
+        first = max(first, 1)
+        all_of(first, last, mix_out, mix_in, all_send.at[1 + n], all_recv.at[1 + n]).wait_send()
+        for half in range(2):
+            all_of(
+                first, last, ret_out.at[half], ret_in.at[half], all_send.at[3 + 2 * n + half],
+                all_recv.at[3 + 2 * n + half],
+            ).wait_send()
 
 
 def local(
@@ -536,31 +582,32 @@
         pltpu.VMEM((2, 2, 8, NL), F32),
         pltpu.VMEM((2, 2, 8, NL), F32),
         pltpu.VMEM((8, NL), F32),
-        pltpu.VMEM((3, 8, 896), F32),
-        pltpu.VMEM((3, 4, 8, 896), F32),
+        pltpu.VMEM((3, 16, 448), BF16),
+        pltpu.VMEM((3, 4, 16, 448), BF16),
         pltpu.VMEM((2, 64, 512), BF16),
         pltpu.VMEM((64, 512), BF16),
-        pltpu.VMEM((2, 128, 16, 128), BF16),
-        pltpu.VMEM((2, 128, 16, 128), BF16),
+        pltpu.VMEM((128, 2, 16, 128), BF16),
+        pltpu.VMEM((128, 2, 16, 128), BF16),
         pltpu.VMEM((128, 16, 128), BF16),
         pltpu.VMEM((128, 16, 128), BF16),
         pltpu.VMEM((2, 128, 16, 128), BF16),
         pltpu.VMEM((2, 128, 16, 128), BF16),
         pltpu.VMEM((2, 128, 1024), BF16),
-        pltpu.VMEM((256, 2048), BF16),
-        pltpu.VMEM((256, 1024), BF16),
-        pltpu.VMEM((256, 2048), BF16),
-        pltpu.VMEM((256, 2048), BF16),
-        pltpu.VMEM((256, 1408), BF16),
-        pltpu.VMEM((2, 128, 1024), BF16),
+        pltpu.VMEM((2, 128, 2048), BF16),
+        pltpu.VMEM((128, 1024), BF16),
+        pltpu.VMEM((128, 2048), BF16),
+        pltpu.VMEM((128, 2048), BF16),
+        pltpu.VMEM((128, 1408), BF16),
+        pltpu.VMEM((2, 64, 1024), BF16),
         pltpu.VMEM((64, 2048), BF16),
         pltpu.SemaphoreType.DMA((21,)),
         pltpu.SemaphoreType.DMA((3, 4)),
         pltpu.SemaphoreType.DMA((3, 4)),
         pltpu.SemaphoreType.DMA,
         pltpu.SemaphoreType.DMA,
-        pltpu.SemaphoreType.DMA((5,)),
-        pltpu.SemaphoreType.DMA((5,)),
+        pltpu.SemaphoreType.DMA((7,)),
+        pltpu.SemaphoreType.DMA((7,)),
+        pltpu.SemaphoreType.REGULAR((3,)),
     ]
     return pl.pallas_call(
         layer_kernel,

time: 78.4 us -> 66.2 us (0.84)
  Pallas kernels: 76.6 us -> 64.3 us
    pallas_call x1, Pallas kernels: 76.6 us -> 64.3 us  [local(): pl.pallas_call(layer_kernel, out_shape=jax.ShapeDtypeStruct((64, 2048), B...]
where the time goes in v2:
time: 66.2 us; the launch traced here: 66 us
  Pallas kernels  64.3 us (97%)
  local copies, waits for them, and re-layouts  1.67 us (3%)
    pallas_call x1, Pallas kernels, local(): pl.pallas_call(layer_kernel, out_shape=jax.ShapeDtypeStruct((64, 2048), B...  64.3 us
    unnamed x1, local copies, waits for them, and re-layouts  1.67 us

profile of v2, /device:TPU:1, one launch (start us, length us, event | category | flops | bytes accessed | tf_op | source)
XLA Modules:
  0.0 66.0 jit_solution(13586814529237488965)
XLA Ops:
  0.0 64.3 %layer.1 = bf16[64,2048]{1,0:T(8,128)(2,1)} custom-call(bf16[128,256]{1,0:T(8,128)(2,1)} %refs_0_.1, bf16[128,256]{1,0:T(8,128)(2,1)} %refs_1_.1, f32[2,2,16,64]{3,2,1,0:T(8,128)} %refs_2_.1, f32[2,2,16,32]{3,2,1,0:T(8,128)} %refs_3_.1, f32[2,2,16]{2,1,0:T(2,128)} %refs_4_.1, f32[64,128]{1,0:T(8,128)} %bitcast.15, f32[2,2,256,64]{3,2,1,0:T(8,128)} %bitcast.10, ...), custom_call_target="tpu_custom_call" | custom-call | tf_op jit(solution)/shard_map/layer/pallas_call | solution.py:612
  64.4 1.7 %copy.23 = bf16[64,2048]{1,0:T(8,128)(2,1)} copy(bf16[64,2048]{1,0:T(8,128)(2,1)} %layer.1) | data formatting | bytes 524288

commit v3 on v2

--- a/solution.py
+++ b/solution.py
@@ -17,8 +17,8 @@
 NL = 1536
 SETS = ((64, 0), (32, 1024))
 CHUNK = 512
-BATCHES = ((1, 31), (31, 61), (61, 91), (91, 128))
-PARTS = ((0, 64), (64, 128))
+BATCHES = ((97, 128), (65, 97), (33, 65), (1, 33))
+PARTS = ((64, 128), (0, 64))
 
 
 def dot(a, b):
@@ -49,41 +49,24 @@
     return ar * ar - ai * ai, 2.0 * ar * ai
 
 
-def coords():
-    return [lax.axis_index(a) for a in SP_TP]
-
-
-def partner(o, way=1):
-    o = lax.rem(o * 37, 128)
-    steps = (o // 32, lax.rem(o // 8, 4), lax.rem(o // 2, 4), lax.rem(o, 2))
-    sizes = (4, 4, 4, 2)
-    there = [lax.rem(p + n + way * s, n) for p, s, n in zip(coords(), steps, sizes)]
-    number = ((there[0] * 4 + there[1]) * 4 + there[2]) * 2 + there[3]
-    return dict(zip(SP_TP, there)), number
-
-
-def send_some(first, last, out, arrived, send_sem, recv_sem):
-    def one(o, carry):
-        where, _ = partner(o)
+def scattered():
+    steps = [(o // 32, o // 8 % 4, o // 2 % 4, o % 2) for o in range(128)]
+    return [steps[o] for o in sorted(range(128), key=lambda o: (o > 0, o * 37 % 128))]
+
+
+STEPS = scattered()
+SIZES = (4, 4, 4, 2)
+
+
+def send_some(first, last, out, arrived, send_sem, recv_sem, way=1):
+    there = [
+        [lax.rem(lax.axis_index(a) + n + way * s, n) for s in range(n)] for a, n in zip(SP_TP, SIZES)
+    ]
+    for o in reversed(range(max(first, 1), last)):
         pltpu.make_async_remote_copy(
             src_ref=out.at[o], dst_ref=arrived.at[o], send_sem=send_sem, recv_sem=recv_sem,
-            device_id=where, device_id_type=MESH,
+            device_id={a: there[k][STEPS[o][k]] for k, a in enumerate(SP_TP)}, device_id_type=MESH,
         ).start()
-        return carry
-
-    lax.fori_loop(first, last, one, 0)
-
-
-def send_back(first, last, out, arrived, send_sem, recv_sem):
-    def one(o, carry):
-        where, _ = partner(o, -1)
-        pltpu.make_async_remote_copy(
-            src_ref=out.at[o], dst_ref=arrived.at[o], send_sem=send_sem, recv_sem=recv_sem,
-            device_id=where, device_id_type=MESH,
-        ).start()
-        return carry
-
-    lax.fori_loop(first, last, one, 0)
 
 
 def all_of(first, last, out, arrived, send_sem, recv_sem):
@@ -125,11 +108,11 @@
 
 
 def layer_kernel(*refs):
-    ins, out_ref, held = refs[:21], refs[21], refs[22 : 22 + 21]
+    ins, out_ref, held = refs[:23], refs[23], refs[24 : 24 + 23]
     (win_w, win_n, wout_w, wout_n, xs, es, spread, carry_ref, prod_ref, lam_ref, send, recv, mine, theirs,
      res_out, res_in, mix_out, mix_in, ret_out, ret_in, slots, rows_ref, mixed_ref, hidden_ref, normed_ref, inner_ref,
      back_ref, own_ref,
-     load_sem, send_sem, recv_sem, tp_send, tp_recv, all_send, all_recv, known_sem) = refs[43:]
+     load_sem, send_sem, recv_sem, tp_send, tp_recv, all_send, all_recv, known_sem) = refs[47:]
     axes = ("sp_2", "sp_1", "sp_0")
     pos = [lax.axis_index(a) for a in axes]
     core = lax.axis_index("tp")
@@ -144,45 +127,50 @@
         greet(barrier, a, p, 4)
     greet(barrier, "tp", core, 2)
     loads = [pltpu.make_async_copy(a, b, load_sem.at[k]) for k, (a, b) in enumerate(zip(ins, held))]
-    order = [12, 16, 2, 3, 4, 6, 7, 8, 9, 0, 1, 5, 10, 11, 13, 15, 17, 14, 18, 19, 20]
-    for k in order[:17]:
+    order = [2, 3, 4, 6, 7, 0, 1, 5, 16, 12, 21, 22, 8, 9, 10, 11, 13, 15, 17, 14, 18, 19, 20]
+    for k in order[:19]:
         loads[k].start()
     (uw_ref, un_ref, pw_ref, pn_ref, step_ref, forget_ref, inw_ref, inn_ref, ow_ref, on_ref,
      skip_ref, gate_ref, residual_ref, mgain_ref, outp_ref, fgain_ref, routes_ref, weights_ref,
-     wg_ref, wu_ref, wd_ref) = held
-    for k in order[:17]:
+     wg_ref, wu_ref, wd_ref, down_ref, across_ref) = held
+    for k in order[:19]:
         loads[k].wait()
-    for k in order[17:]:
+    for k in order[19:]:
         loads[k].start()
 
     swap = swap_matrix()
     earlier = (iota((64, 64), 0) < iota((64, 64), 1)).astype(BF16)
-    expert = partner(iota((128, 64), 0))[1]
+    def numbers(steps):
+        there = [lax.rem(lax.axis_index(a) + t, n) for a, t, n in zip(SP_TP, steps, SIZES)]
+        return ((there[0] * 4 + there[1]) * 4 + there[2]) * 2 + there[3]
+
+    expert = numbers([down_ref[:, k : k + 1] for k in range(4)])
     named = [(expert == routes_ref[k : k + 1, :]).astype(F32) for k in range(2)]
     count = named[0] + named[1]
     rank = dot(count.astype(BF16), earlier)
     pick = [jnp.where(rank == r, count, 0.0).astype(BF16) for r in range(2)]
-    for half in range(2):
-        for r in range(2):
-            slots[r] = dot(pick[r], residual_ref[:, half * 1024 : (half + 1) * 1024]).astype(BF16)
-
-        def put_residual(at, block):
-            res_out[at : at + 16, half] = block
-
-        pack(lambda r, at, j: slots[r, at : at + 16, j * 128 : (j + 1) * 128], swap, put_residual, 128)
     pl.semaphore_wait(barrier, 10)
     greet(known_sem.at[0], "sp_2", pos[0], 4)
+
+    def spreader(n):
+        tiler = (iota((n, 8 * n), 0) == lax.rem(iota((n, 8 * n), 1), n)).astype(BF16)
+        return tiler, iota((128, 8 * n), 0) // 16 == iota((128, 8 * n), 1) // n
+
+    def build_out():
+        for n, o_ref, wout in ((64, ow_ref, wout_w), (32, on_ref, wout_n)):
+            tiler, keep = spreader(n)
+            for d in range(2):
+                for ri in range(2):
+                    for h in range(2):
+                        o = o_ref[d, ri, h * 128 : (h + 1) * 128, :]
+                        o = (-o if ri else o).astype(BF16)
+                        wout[d, ri, h] = jnp.where(keep, dot(o, tiler), 0.0).astype(BF16)
 
     for s, (p_ref, in_ref, o_ref, win, wout) in enumerate(
         ((pw_ref, inw_ref, ow_ref, win_w, wout_w), (pn_ref, inn_ref, on_ref, win_n, wout_n))
     ):
         n, first = SETS[s]
-        tile_r = iota((n, 8 * n), 0)
-        tile_c = iota((n, 8 * n), 1)
-        tiler = (tile_r == lax.rem(tile_c, n)).astype(BF16)
-        wr = iota((128, 8 * n), 0)
-        wc = iota((128, 8 * n), 1)
-        keep = (wr // 16) == (wc // n)
+        tiler, keep = spreader(n)
         for d in range(2):
             pr = p_ref[d, 0]
             pi = p_ref[d, 1]
@@ -213,9 +201,6 @@
                 for ri, rows in ((0, ere), (1, eim)):
                     part = jnp.concatenate(rows[8 * h : 8 * h + 8], axis=0)
                     win[d, ri, h] = jnp.where(keep, dot(part, tiler), 0.0).astype(BF16)
-                    o = o_ref[d, ri, h * 128 : (h + 1) * 128, :]
-                    o = (-o if ri else o).astype(BF16)
-                    wout[d, ri, h] = jnp.where(keep, dot(o, tiler), 0.0).astype(BF16)
 
     pl.semaphore_wait(known_sem.at[0], 3)
     greet(known_sem.at[1], "sp_1", pos[1], 4)
@@ -334,6 +319,16 @@
                 )
             )
             copies[-1].start()
+        if stage == 0:
+            build_out()
+            for half in range(2):
+                for r in range(2):
+                    slots[r] = dot(pick[r], residual_ref[:, half * 1024 : (half + 1) * 1024]).astype(BF16)
+
+                def put_residual(at, block):
+                    res_out[at : at + 16, half] = block
+
+                pack(lambda r, at, j: slots[r, at : at + 16, j * 128 : (j + 1) * 128], swap, put_residual, 128)
         send_some(*BATCHES[stage], res_out, res_in, all_send.at[0], all_recv.at[0])
         for o in (1, 3, 2):
             there = lax.rem(p + o, 4)
@@ -444,7 +439,7 @@
 
     pack(lambda r, at, j: slots[r, at : at + 16, j * 128 : (j + 1) * 128], swap, put_mixed_out, 128)
     for n, (first, last) in enumerate(PARTS):
-        send_some(max(first, 1), last, mix_out, mix_in, all_send.at[1 + n], all_recv.at[1 + n])
+        send_some(first, last, mix_out, mix_in, all_send.at[1 + n], all_recv.at[1 + n])
     mix_in[0] = mix_out[0]
 
     loads[14].wait()
@@ -466,7 +461,7 @@
     eye = iota((64, 64), 0) == iota((64, 64), 1)
     def column(row):
         return jnp.sum(jnp.where(eye, row, 0.0), axis=1, keepdims=True)
-    experts = partner(iota((64, 128), 1))[1].astype(F32)
+    experts = numbers([across_ref[k : k + 1, :] for k in range(4)]).astype(F32)
     hits = [(column(routes_ref[k : k + 1, :].astype(F32)) == experts).astype(F32) for k in range(2)]
     w = [column(weights_ref[k : k + 1, :]) for k in range(2)]
     both = w[0] + w[1]
@@ -479,7 +474,7 @@
         first = share.astype(BF16)
         parts.append((first, (share - first.astype(F32)).astype(BF16)))
 
-    for k in order[18:]:
+    for k in order[20:]:
         loads[k].wait()
     for n, (first, last) in enumerate(PARTS):
         all_of(max(first, 1), last, mix_out, mix_in, all_send.at[1 + n], all_recv.at[1 + n]).wait_recv()
@@ -517,28 +512,21 @@
                     slots[r, 0:64, c * 256 : (c + 1) * 256] = y[r * 64 : (r + 1) * 64]
 
             def put_return(at, block):
-                ret_out[half, first + at : first + at + 16] = block
+                ret_out[first + at : first + at + 16, half] = block
 
             pack(lambda r, at, j: slots[r, at : at + 16, j * 128 : (j + 1) * 128], swap, put_return, 64)
-            send_back(
-                max(first, 1), last, ret_out.at[half], ret_in.at[half], all_send.at[3 + 2 * n + half],
-                all_recv.at[3 + 2 * n + half],
-            )
-    for half in range(2):
-        ret_in[half, 0] = ret_out[half, 0]
+        send_some(first, last, ret_out, ret_in, all_send.at[3 + n], all_recv.at[3 + n], -1)
+    ret_in[0] = ret_out[0]
 
     y = [own_ref[:, c * 256 : (c + 1) * 256].astype(F32) for c in range(8)]
     for n, (first, last) in enumerate(PARTS):
+        all_of(max(first, 1), last, ret_out, ret_in, all_send.at[3 + n], all_recv.at[3 + n]).wait_recv()
         for half in range(2):
-            all_of(
-                max(first, 1), last, ret_out.at[half], ret_in.at[half], all_send.at[3 + 2 * n + half],
-                all_recv.at[3 + 2 * n + half],
-            ).wait_recv()
 
             def put_back(r, at, j, rows):
                 back_ref[r, at : at + 16, j * 128 : (j + 1) * 128] = rows
 
-            unpack(lambda at: ret_in[half, first + at : first + at + 16], swap, put_back, 64)
+            unpack(lambda at: ret_in[first + at : first + at + 16, half], swap, put_back, 64)
             for c in range(4):
                 lanes = slice(c * 256, (c + 1) * 256)
                 for r in range(2):
@@ -551,11 +539,7 @@
     for n, (first, last) in enumerate(PARTS):
         first = max(first, 1)
         all_of(first, last, mix_out, mix_in, all_send.at[1 + n], all_recv.at[1 + n]).wait_send()
-        for half in range(2):
-            all_of(
-                first, last, ret_out.at[half], ret_in.at[half], all_send.at[3 + 2 * n + half],
-                all_recv.at[3 + 2 * n + half],
-            ).wait_send()
+        all_of(first, last, ret_out, ret_in, all_send.at[3 + n], all_recv.at[3 + n]).wait_send()
 
 
 def local(
@@ -569,6 +553,7 @@
         wide_out_map.reshape(2, 2, 256, 64), narrow_out_map.reshape(2, 2, 256, 32),
         skip_weight, gate_mix.reshape(2, 256, 16), residual, mixer_gain.reshape(1, 1024), out_proj,
         ffn_gain.reshape(1, 2048), routes.T, route_weights.T, gate_proj, up_proj, down_proj,
+        jnp.asarray(STEPS, jnp.int32), jnp.asarray(STEPS, jnp.int32).T,
     )
     scratch = [pltpu.VMEM(a.shape, a.dtype) for a in ins]
     scratch += [
@@ -590,8 +575,8 @@
         pltpu.VMEM((128, 2, 16, 128), BF16),
         pltpu.VMEM((128, 16, 128), BF16),
         pltpu.VMEM((128, 16, 128), BF16),
-        pltpu.VMEM((2, 128, 16, 128), BF16),
-        pltpu.VMEM((2, 128, 16, 128), BF16),
+        pltpu.VMEM((128, 2, 16, 128), BF16),
+        pltpu.VMEM((128, 2, 16, 128), BF16),
         pltpu.VMEM((2, 128, 1024), BF16),
         pltpu.VMEM((2, 128, 2048), BF16),
         pltpu.VMEM((128, 1024), BF16),
@@ -600,7 +585,7 @@
         pltpu.VMEM((128, 1408), BF16),
         pltpu.VMEM((2, 64, 1024), BF16),
         pltpu.VMEM((64, 2048), BF16),
-        pltpu.SemaphoreType.DMA((21,)),
+        pltpu.SemaphoreType.DMA((23,)),
         pltpu.SemaphoreType.DMA((3, 4)),
         pltpu.SemaphoreType.DMA((3, 4)),
         pltpu.SemaphoreType.DMA,
@@ -612,7 +597,7 @@
     return pl.pallas_call(
         layer_kernel,
         out_shape=jax.ShapeDtypeStruct((64, 2048), BF16),
-        in_specs=[pl.BlockSpec(memory_space=pl.ANY)] * 21,
+        in_specs=[pl.BlockSpec(memory_space=pl.ANY)] * 23,
         out_specs=pl.BlockSpec(memory_space=pltpu.VMEM),
         scratch_shapes=scratch,
         compiler_params=pltpu.CompilerParams(

time: 66.2 us -> 62.9 us (0.950)
  Pallas kernels: 64.3 us -> 61.1 us
    pallas_call x1, Pallas kernels: 64.3 us -> 61.1 us  [local(): pl.pallas_call(layer_kernel, out_shape=jax.ShapeDtypeStruct((64, 2048), B...]
where the time goes in v3:
time: 62.9 us; the launch traced here: 62.8 us
  Pallas kernels  61.1 us (97%)
  local copies, waits for them, and re-layouts  1.67 us (3%)
    pallas_call x1, Pallas kernels, local(): pl.pallas_call(layer_kernel, out_shape=jax.ShapeDtypeStruct((64, 2048), B...  61.1 us
    unnamed x1, local copies, waits for them, and re-layouts  1.67 us

profile of v3, /device:TPU:1, one launch (start us, length us, event | category | flops | bytes accessed | tf_op | source)
XLA Modules:
  0.0 62.8 jit_solution(12579047642300462054)
XLA Ops:
  0.0 61.1 %layer.1 = bf16[64,2048]{1,0:T(8,128)(2,1)} custom-call(bf16[128,256]{1,0:T(8,128)(2,1)} %refs_0_.1, bf16[128,256]{1,0:T(8,128)(2,1)} %refs_1_.1, f32[2,2,16,64]{3,2,1,0:T(8,128)} %refs_2_.1, f32[2,2,16,32]{3,2,1,0:T(8,128)} %refs_3_.1, f32[2,2,16]{2,1,0:T(2,128)} %refs_4_.1, f32[64,128]{1,0:T(8,128)} %bitcast.15, f32[2,2,256,64]{3,2,1,0:T(8,128)} %bitcast.10, ...), custom_call_target="tpu_custom_call" | custom-call | tf_op jit(solution)/shard_map/layer/pallas_call | solution.py:597
  61.1 1.7 %copy.25 = bf16[64,2048]{1,0:T(8,128)(2,1)} copy(bf16[64,2048]{1,0:T(8,128)(2,1)} %layer.1) | data formatting | bytes 524288

commit v4 on v3

--- a/solution.py
+++ b/solution.py
@@ -17,7 +17,7 @@
 NL = 1536
 SETS = ((64, 0), (32, 1024))
 CHUNK = 512
-BATCHES = ((97, 128), (65, 97), (33, 65), (1, 33))
+BATCHES = ((108, 128), (86, 108), (62, 86), (1, 62))
 PARTS = ((64, 128), (0, 64))
 
 
@@ -133,24 +133,8 @@
     (uw_ref, un_ref, pw_ref, pn_ref, step_ref, forget_ref, inw_ref, inn_ref, ow_ref, on_ref,
      skip_ref, gate_ref, residual_ref, mgain_ref, outp_ref, fgain_ref, routes_ref, weights_ref,
      wg_ref, wu_ref, wd_ref, down_ref, across_ref) = held
-    for k in order[:19]:
+    for k in order[:8]:
         loads[k].wait()
-    for k in order[19:]:
-        loads[k].start()
-
-    swap = swap_matrix()
-    earlier = (iota((64, 64), 0) < iota((64, 64), 1)).astype(BF16)
-    def numbers(steps):
-        there = [lax.rem(lax.axis_index(a) + t, n) for a, t, n in zip(SP_TP, steps, SIZES)]
-        return ((there[0] * 4 + there[1]) * 4 + there[2]) * 2 + there[3]
-
-    expert = numbers([down_ref[:, k : k + 1] for k in range(4)])
-    named = [(expert == routes_ref[k : k + 1, :]).astype(F32) for k in range(2)]
-    count = named[0] + named[1]
-    rank = dot(count.astype(BF16), earlier)
-    pick = [jnp.where(rank == r, count, 0.0).astype(BF16) for r in range(2)]
-    pl.semaphore_wait(barrier, 10)
-    greet(known_sem.at[0], "sp_2", pos[0], 4)
 
     def spreader(n):
         tiler = (iota((n, 8 * n), 0) == lax.rem(iota((n, 8 * n), 1), n)).astype(BF16)
@@ -202,8 +186,12 @@
                     part = jnp.concatenate(rows[8 * h : 8 * h + 8], axis=0)
                     win[d, ri, h] = jnp.where(keep, dot(part, tiler), 0.0).astype(BF16)
 
-    pl.semaphore_wait(known_sem.at[0], 3)
-    greet(known_sem.at[1], "sp_1", pos[1], 4)
+    for k in order[8:19]:
+        loads[k].wait()
+    for k in order[19:]:
+        loads[k].start()
+    pl.semaphore_wait(barrier, 10)
+    greet(known_sem.at[0], "sp_2", pos[0], 4)
     pr_ = iota((128, 128), 0)
     pc_ = iota((128, 128), 1)
     perm = (pc_ == lax.rem(pr_, 8) * 16 + pr_ // 8).astype(BF16)
@@ -244,8 +232,6 @@
             new += [nre, nim, state[3 * d + 2] if keep_states else state[3 * d + 2] * e]
         return tuple(new)
 
-    pl.semaphore_wait(known_sem.at[1], 3)
-    greet(known_sem.at[2], "tp", core, 2)
     sub = iota((8, CHUNK), 0)
     ends = [[], []]
     for c in range(NL // CHUNK):
@@ -295,7 +281,8 @@
     ]
     power = [[lam_ref[4 + 2 * d + q : 5 + 2 * d + q, :] for q in range(2)] for d in range(2)]
     enter = None
-    pl.semaphore_wait(known_sem.at[2], 1)
+    pl.semaphore_wait(known_sem.at[0], 3)
+    greet(known_sem.at[1], "sp_1", pos[1], 4)
     for stage, a in enumerate(axes):
         p = pos[stage]
         lines = [
@@ -321,6 +308,17 @@
             copies[-1].start()
         if stage == 0:
             build_out()
+            swap = swap_matrix()
+            earlier = (iota((64, 64), 0) < iota((64, 64), 1)).astype(BF16)
+            def numbers(steps):
+                there = [lax.rem(lax.axis_index(a) + t, n) for a, t, n in zip(SP_TP, steps, SIZES)]
+                return ((there[0] * 4 + there[1]) * 4 + there[2]) * 2 + there[3]
+
+            expert = numbers([down_ref[:, k : k + 1] for k in range(4)])
+            named = [(expert == routes_ref[k : k + 1, :]).astype(F32) for k in range(2)]
+            count = named[0] + named[1]
+            rank = dot(count.astype(BF16), earlier)
+            pick = [jnp.where(rank == r, count, 0.0).astype(BF16) for r in range(2)]
             for half in range(2):
                 for r in range(2):
                     slots[r] = dot(pick[r], residual_ref[:, half * 1024 : (half + 1) * 1024]).astype(BF16)
@@ -329,6 +327,9 @@
                     res_out[at : at + 16, half] = block
 
                 pack(lambda r, at, j: slots[r, at : at + 16, j * 128 : (j + 1) * 128], swap, put_residual, 128)
+            pl.semaphore_wait(known_sem.at[1], 3)
+            greet(known_sem.at[2], "tp", core, 2)
+            pl.semaphore_wait(known_sem.at[2], 1)
         send_some(*BATCHES[stage], res_out, res_in, all_send.at[0], all_recv.at[0])
         for o in (1, 3, 2):
             there = lax.rem(p + o, 4)
@@ -431,14 +432,14 @@
     joined = jnp.concatenate([low[:, :256], high[:, :256], low[:, 256:], high[:, 256:]], axis=1)
     scale = lax.rsqrt(jnp.mean(joined * joined, axis=1, keepdims=True) + epsilon)
     mixed = (joined * scale * mgain_ref[...]).astype(BF16)
-    for r in range(2):
-        slots[r] = dot(pick[r], mixed).astype(BF16)
-
-    def put_mixed_out(at, block):
-        mix_out[at : at + 16] = block
-
-    pack(lambda r, at, j: slots[r, at : at + 16, j * 128 : (j + 1) * 128], swap, put_mixed_out, 128)
     for n, (first, last) in enumerate(PARTS):
+        for r in range(2):
+            slots[r, 0:64] = dot(pick[r][first:last], mixed).astype(BF16)
+
+        def put_mixed_out(at, block):
+            mix_out[first + at : first + at + 16] = block
+
+        pack(lambda r, at, j: slots[r, at : at + 16, j * 128 : (j + 1) * 128], swap, put_mixed_out, 64)
         send_some(first, last, mix_out, mix_in, all_send.at[1 + n], all_recv.at[1 + n])
     mix_in[0] = mix_out[0]
 

time: 62.9 us -> 60.4 us (0.960)
  Pallas kernels: 61.1 us -> 58.6 us
    pallas_call x1, Pallas kernels: 61.1 us -> 58.6 us  [local(): pl.pallas_call(layer_kernel, out_shape=jax.ShapeDtypeStruct((64, 2048), B...]
where the time goes in v4:
time: 60.4 us; the launch traced here: 60.3 us
  Pallas kernels  58.6 us (97%)
  local copies, waits for them, and re-layouts  1.67 us (3%)
    pallas_call x1, Pallas kernels, local(): pl.pallas_call(layer_kernel, out_shape=jax.ShapeDtypeStruct((64, 2048), B...  58.6 us
    unnamed x1, local copies, waits for them, and re-layouts  1.67 us

profile of v4, /device:TPU:1, one launch (start us, length us, event | category | flops | bytes accessed | tf_op | source)
XLA Modules:
  0.0 60.3 jit_solution(6974567937953882187)
XLA Ops:
  0.0 58.6 %layer.1 = bf16[64,2048]{1,0:T(8,128)(2,1)} custom-call(bf16[128,256]{1,0:T(8,128)(2,1)} %refs_0_.1, bf16[128,256]{1,0:T(8,128)(2,1)} %refs_1_.1, f32[2,2,16,64]{3,2,1,0:T(8,128)} %refs_2_.1, f32[2,2,16,32]{3,2,1,0:T(8,128)} %refs_3_.1, f32[2,2,16]{2,1,0:T(2,128)} %refs_4_.1, f32[64,128]{1,0:T(8,128)} %bitcast.15, f32[2,2,256,64]{3,2,1,0:T(8,128)} %bitcast.10, ...), custom_call_target="tpu_custom_call" | custom-call | tf_op jit(solution)/shard_map/layer/pallas_call | solution.py:598
  58.6 1.7 %copy.25 = bf16[64,2048]{1,0:T(8,128)(2,1)} copy(bf16[64,2048]{1,0:T(8,128)(2,1)} %layer.1) | data formatting | bytes 524288

commit v5 on v4

--- a/solution.py
+++ b/solution.py
@@ -281,6 +281,7 @@
     ]
     power = [[lam_ref[4 + 2 * d + q : 5 + 2 * d + q, :] for q in range(2)] for d in range(2)]
     enter = None
+    carry_copies = []
     pl.semaphore_wait(known_sem.at[0], 3)
     greet(known_sem.at[1], "sp_1", pos[1], 4)
     for stage, a in enumerate(axes):
@@ -306,8 +307,9 @@
                 )
             )
             copies[-1].start()
+        if stage == 1:
+            build_out()
         if stage == 0:
-            build_out()
             swap = swap_matrix()
             earlier = (iota((64, 64), 0) < iota((64, 64), 1)).astype(BF16)
             def numbers(steps):
@@ -379,8 +381,7 @@
                 ncre, ncim = cmul(cre, cim, jre, jim)
                 enter[d] = [bre + add_re, bim + add_im, ncre, ncim]
         fsum = jnp.sum(sums, axis=0, keepdims=True)
-        for copy in copies:
-            copy.wait_send()
+        carry_copies += copies
 
     send_some(*BATCHES[3], res_out, res_in, all_send.at[0], all_recv.at[0])
     res_in[0] = res_out[0]
@@ -424,7 +425,7 @@
         device_id_type=MESH,
     )
     copy.start()
-    copy.wait()
+    copy.wait_recv()
 
     own, other = mine[core].astype(F32), theirs[...].astype(F32)
     low = jnp.where(core == 0, own, other)
@@ -536,6 +537,9 @@
     for c in range(8):
         out_ref[:, c * 256 : (c + 1) * 256] = y[c].astype(BF16)
 
+    copy.wait_send()
+    for copy in carry_copies:
+        copy.wait_send()
     all_of(1, 128, res_out, res_in, all_send.at[0], all_recv.at[0]).wait_send()
     for n, (first, last) in enumerate(PARTS):
         first = max(first, 1)

time: 60.4 us -> 59 us (0.977)
  Pallas kernels: 58.6 us -> 57.2 us
    pallas_call x1, Pallas kernels: 58.6 us -> 57.2 us  [local(): pl.pallas_call(layer_kernel, out_shape=jax.ShapeDtypeStruct((64, 2048), B...]
where the time goes in v5:
time: 59 us; the launch traced here: 58.9 us
  Pallas kernels  57.2 us (97%)
  local copies, waits for them, and re-layouts  1.67 us (3%)
    pallas_call x1, Pallas kernels, local(): pl.pallas_call(layer_kernel, out_shape=jax.ShapeDtypeStruct((64, 2048), B...  57.2 us
    unnamed x1, local copies, waits for them, and re-layouts  1.67 us

profile of v5, /device:TPU:1, one launch (start us, length us, event | category | flops | bytes accessed | tf_op | source)
XLA Modules:
  0.0 58.9 jit_solution(13562970594066049398)
XLA Ops:
  0.0 57.2 %layer.1 = bf16[64,2048]{1,0:T(8,128)(2,1)} custom-call(bf16[128,256]{1,0:T(8,128)(2,1)} %refs_0_.1, bf16[128,256]{1,0:T(8,128)(2,1)} %refs_1_.1, f32[2,2,16,64]{3,2,1,0:T(8,128)} %refs_2_.1, f32[2,2,16,32]{3,2,1,0:T(8,128)} %refs_3_.1, f32[2,2,16]{2,1,0:T(2,128)} %refs_4_.1, f32[64,128]{1,0:T(8,128)} %bitcast.15, f32[2,2,256,64]{3,2,1,0:T(8,128)} %bitcast.10, ...), custom_call_target="tpu_custom_call" | custom-call | tf_op jit(solution)/shard_map/layer/pallas_call | solution.py:602
  57.2 1.7 %copy.25 = bf16[64,2048]{1,0:T(8,128)(2,1)} copy(bf16[64,2048]{1,0:T(8,128)(2,1)} %layer.1) | data formatting | bytes 524288
